TPU v7x, 128 devices: a whole 4x4x4 slice. The times are simulated.
128 devices in a mesh: ep: 32 (over z, y, core), tp: 4 (over x).
Axes of the slice: x: 4, y: 4, z: 4, core: 2. Of those that a mesh axis runs over, the one named last changes fastest.
Arguments:
- q_latent: bfloat16 [16384, 1024], P(('ep', 'tp')), may hold values from -6 to 6
- kv_latent: bfloat16 [16384, 512], P(('ep', 'tp')), may hold values from -8 to 8
- rope_key: bfloat16 [16384, 64], P(('ep', 'tp')), may hold values from -2500 to 2500
- gain_query: float32 [1024], replicated, may hold values from 0.1 to 1.9
- gain_latent: float32 [512], replicated, may hold values from 0.1 to 1.9
- w_query: bfloat16 [1024, 3072], P(None, 'tp'), may hold values from -0.1875 to 0.1875
- w_key: bfloat16 [512, 2048], P(None, 'tp'), may hold values from -0.625 to 0.625
- w_value: bfloat16 [512, 2048], P(None, 'tp'), may hold values from -0.25 to 0.25
- w_out: bfloat16 [2048, 4096], P('tp'), may hold values from -0.25 to 0.25
- tokens_b: bfloat16 [16384, 4096], P(('ep', 'tp')), may hold values from -6 to 6
- gain_norm: float32 [4096], replicated, may hold values from 0.1 to 1.9
- routes: int32 [16384, 2], P(('ep', 'tp')), may hold values from 0 to 31, all different within a row; in each aligned block of 128 rows (0 to 127, 128 to 255, ...) at most 10 rows name the same one
- route_weights: float32 [16384, 2], P(('ep', 'tp')), may hold values from 0.2 to 1
- shared_gate: bfloat16 [4096, 1024], P(None, 'tp'), may hold values from -0.09375 to 0.09375
- shared_up: bfloat16 [4096, 1024], P(None, 'tp'), may hold values from -0.09375 to 0.09375
- shared_down: bfloat16 [1024, 4096], P('tp'), may hold values from -0.1875 to 0.1875
- expert_gate: bfloat16 [32, 4096, 1024], P('ep', None, 'tp'), may hold values from -0.09375 to 0.09375
- expert_up: bfloat16 [32, 4096, 1024], P('ep', None, 'tp'), may hold values from -0.09375 to 0.09375
- expert_down: bfloat16 [32, 1024, 4096], P('ep', 'tp'), may hold values from -0.1875 to 0.1875
Outputs:
- mixer_out: bfloat16 [16384, 4096], P(('ep', 'tp'))
- expert_mix: bfloat16 [16384, 4096], P(('ep', 'tp'))
Inputs may be any that keep to these rules, and one draw needn't show every extreme that they name: `routes`: in each aligned block of 128 rows no expert is named by more than 10 rows.
All inputs are finite; a program needn't handle non-finite values.
Results may differ from a plain program's by a relative error of at most 0.018.
The roundings to bfloat16 on the way count: a program that leaves them out, or rounds other values in their place, can miss the bound.
Values may be sent and summed in bfloat16 or wider, within the bound.
No kernel may reach another device: no remote copies, remote signals or barrier semaphores. Data moves between devices by JAX's collectives and lax.ppermute only.
A program may use at most 192 MiB of HBM per device.

v0:
```python
import jax
import jax.numpy as jnp
from jax import lax
from jax.sharding import Mesh
from jax.sharding import PartitionSpec as P

NOPE = 128
ROPE = 64
VDIM = 128
SEQS = 1
EP = ("ep_0", "ep_1", "ep_2")
EP_TP = ("ep_0", "ep_1", "ep_2", "tp")


epsilon = 1e-06
rope_theta = 10000.0


def passed_along(value, axis, steps):
    count = lax.axis_size(axis)
    initial, last = (max(0, -steps), min(count, count - steps))
    return lax.ppermute(value, axis, [(source, source + steps) for source in range(initial, last)])


def split_up(x, dim, count):
    dims = x.shape
    pieces = x.reshape(*dims[:dim], count, dims[dim] // count, *dims[dim + 1 :])
    return jnp.moveaxis(pieces, dim, 0)


def in_order(pieces, dim):
    dims = list(pieces.shape[1:])
    dims[dim] *= pieces.shape[0]
    return jnp.moveaxis(pieces, 0, dim).reshape(dims)


def turned_blocks(pieces, axes, sequence):
    inside = pieces.shape[1:]
    out = pieces.reshape(*(lax.axis_size(a) for a in axes), *inside)
    for k in sequence:
        out = lax.all_to_all(out, axes[k], k, k, tiled=True)
    return out.reshape(-1, *inside)


def two_step_exchange(x, groups, sequence, split_dim, concat_dim):
    count = lax.axis_size(groups[0]) * lax.axis_size(groups[1])
    pieces = split_up(x, split_dim, count)
    return in_order(turned_blocks(pieces, groups, sequence), concat_dim)


def sent_and_summed(x, axis, dim):
    count = lax.axis_size(axis)
    pieces = lax.all_to_all(split_up(x, dim, count), axis, 0, 0, tiled=True)
    return jnp.sum(pieces.astype(jnp.float32), axis=0)


def rms_scale(values, gain_vec):
    floats = values.astype(jnp.float32)
    scaled = floats * lax.rsqrt(jnp.mean(floats * floats, axis=-1, keepdims=True) + epsilon)
    return (scaled * gain_vec).astype(jnp.bfloat16)


def rope_angles(positions, rope_width):
    frequency = rope_theta ** (-jnp.arange(0, rope_width, 2, dtype=jnp.float32) / rope_width)
    angles = positions.astype(jnp.float32)[:, None] * frequency[None, :]
    return (jnp.cos(angles), jnp.sin(angles))


def rotate_pairs(values, cos_tab, sin_tab):
    half_width = values.shape[-1] // 2
    first_half = values[..., :half_width]
    second_half = values[..., half_width:]
    return jnp.concatenate(
        [
            first_half * cos_tab - second_half * sin_tab,
            second_half * cos_tab + first_half * sin_tab,
        ],
        axis=-1,
    )


def block_scores(query_nope, query_rot, kv_block, pe_block, w_key, w_value, head_local):
    key_rows = kv_block.shape[0]
    key_proj = jnp.dot(kv_block, w_key, preferred_element_type=jnp.float32).astype(jnp.bfloat16)
    key_proj = key_proj.reshape(key_rows, head_local, -1)
    values = jnp.dot(kv_block, w_value, preferred_element_type=jnp.float32).astype(jnp.bfloat16)
    values = values.reshape(key_rows, head_local, -1)
    scores = jnp.einsum("qhd,khd->hqk", query_nope, key_proj, preferred_element_type=jnp.float32)
    scores = scores + jnp.einsum(
        "qhr,kr->hqk", query_rot, pe_block, preferred_element_type=jnp.float32
    )
    return (scores * (NOPE + ROPE) ** (-0.5), values)


def absorb(running, scores, values):
    top_old, sum_old, acc_old = running
    top_new = jnp.maximum(top_old, jnp.max(scores, axis=-1))
    factor = jnp.exp(top_old - top_new)
    exp_terms = jnp.exp(scores - top_new[:, :, None])
    sum_new = sum_old * factor + jnp.sum(exp_terms, axis=-1)
    update = jnp.einsum(
        "hqk,khd->qhd", exp_terms.astype(jnp.bfloat16), values, preferred_element_type=jnp.float32
    )
    return (top_new, sum_new, acc_old * factor.T[:, :, None] + update)


def slot_targets(route_ids, expert_total, capacity):
    pair_ids = route_ids.reshape(route_ids.shape[:-2] + (-1,))
    onehot = (pair_ids[..., None] == jnp.arange(expert_total, dtype=jnp.int32)).astype(jnp.int32)
    earlier = jnp.cumsum(onehot, axis=-2) - onehot
    return pair_ids * capacity + jnp.sum(earlier * onehot, axis=-1)


def dispatch_matrix(targets, tok_rows, top_k, slot_total):
    matches = targets[..., None, :] == jnp.arange(slot_total, dtype=jnp.int32)[:, None]
    matches = matches.reshape(matches.shape[:-1] + (tok_rows, top_k))
    return jnp.any(matches, axis=-1).astype(jnp.bfloat16)


def on_device(
    q_latent,
    kv_latent,
    rope_key,
    gain_query,
    gain_latent,
    w_query,
    w_key,
    w_value,
    w_out,
    tokens_b,
    gain_norm,
    routes,
    route_weights,
    shared_gate,
    shared_up,
    shared_down,
    expert_gate,
    expert_up,
    expert_down,
):
    tok_rows = q_latent.shape[0]
    tp_count = lax.axis_size("tp")
    ep_count = lax.axis_size(EP)
    group_rows = tok_rows * tp_count
    seq_span = ep_count // SEQS
    local_rank = lax.axis_index(EP) % seq_span
    head_local = w_value.shape[1] // VDIM
    q_normed = rms_scale(q_latent, gain_query)
    kv_normed = rms_scale(kv_latent, gain_latent)
    group_q, group_kv, group_pe = (
        lax.all_gather(q_normed, "tp", axis=0, tiled=True),
        lax.all_gather(kv_normed, "tp", axis=0, tiled=True),
        lax.all_gather(rope_key, "tp", axis=0, tiled=True),
    )
    positions = local_rank * group_rows + jnp.arange(group_rows, dtype=jnp.int32)
    cos_tab, sin_tab = rope_angles(positions, ROPE)
    query_full = jnp.dot(group_q, w_query, preferred_element_type=jnp.float32)
    query_full = query_full.reshape(group_rows, head_local, NOPE + ROPE)
    query_rot = rotate_pairs(
        query_full[:, :, NOPE:], cos_tab[:, None, :], sin_tab[:, None, :]
    ).astype(jnp.bfloat16)
    query_nope = query_full[:, :, :NOPE].astype(jnp.bfloat16)
    rot_keys = rotate_pairs(group_pe.astype(jnp.float32), cos_tab, sin_tab).astype(jnp.bfloat16)

    def attend(running, kv_block, pe_block):
        scores, values = block_scores(
            query_nope, query_rot, kv_block, pe_block, w_key, w_value, head_local
        )
        return absorb(running, scores, values)

    own_scores, own_values = block_scores(
        query_nope, query_rot, group_kv, rot_keys, w_key, w_value, head_local
    )
    row_ids = jnp.arange(group_rows, dtype=jnp.int32)
    causal = row_ids[:, None] >= row_ids[None, :]
    own_scores = jnp.where(causal[None], own_scores, -jnp.inf)
    start_state = (
        jnp.full((head_local, group_rows), -jnp.inf, jnp.float32),
        jnp.zeros((head_local, group_rows), jnp.float32),
        jnp.zeros((group_rows, head_local, VDIM), jnp.float32),
    )
    running = absorb(start_state, own_scores, own_values)
    held_kv, held_pe = (group_kv, rot_keys)
    level_count = seq_span.bit_length() - 1
    for level_num in range(level_count):
        reach_len = 2**level_num
        recv_kv, recv_pe = passed_along((held_kv, held_pe), EP, reach_len)

        def absorb_block(block_num, held_state):
            kv_block = lax.dynamic_slice_in_dim(recv_kv, block_num * group_rows, group_rows, 0)
            pe_block = lax.dynamic_slice_in_dim(recv_pe, block_num * group_rows, group_rows, 0)
            distance = 2 * reach_len - 1 - block_num
            return lax.cond(
                local_rank >= distance,
                lambda: attend(held_state, kv_block, pe_block),
                lambda: held_state,
            )

        running = lax.fori_loop(0, reach_len, absorb_block, running)
        if level_num + 1 < level_count:
            held_kv = jnp.concatenate([recv_kv, held_kv], axis=0)
            held_pe = jnp.concatenate([recv_pe, held_pe], axis=0)
    sum_all = running[1]
    acc_all = running[2]
    heads_out = (
        (acc_all / sum_all.T[:, :, None])
        .astype(jnp.bfloat16)
        .reshape(group_rows, head_local * VDIM)
    )
    mixer_out = lax.psum_scatter(
        jnp.dot(heads_out, w_out, preferred_element_type=jnp.float32).astype(jnp.bfloat16),
        "tp",
        scatter_dimension=0,
        tiled=True,
    )
    top_k = routes.shape[1]
    model_width = tokens_b.shape[1]
    exp_dev = expert_gate.shape[0]
    expert_total = exp_dev * ep_count
    capacity = 5 * tok_rows * top_k // (4 * expert_total)
    slot_total = expert_total * capacity
    normed_b = rms_scale(tokens_b, gain_norm)
    own_targets = slot_targets(routes, expert_total, capacity)
    mapping = dispatch_matrix(own_targets, tok_rows, top_k, slot_total)
    outgoing = jnp.dot(mapping, normed_b, preferred_element_type=jnp.float32).astype(jnp.bfloat16)
    outgoing = outgoing.reshape(ep_count, exp_dev * capacity, model_width)
    incoming = two_step_exchange(outgoing, (("ep_0", "ep_1"), "ep_2"), (1, 0), 0, 0)
    shared_rows, arrived = (
        lax.all_gather(normed_b, "tp", axis=0, tiled=True),
        lax.all_gather(incoming, "tp", axis=0, tiled=True),
    )
    routed = arrived.reshape(tp_count, ep_count, exp_dev, capacity, model_width)
    gate_shared = jnp.dot(shared_rows, shared_gate, preferred_element_type=jnp.float32)
    up_shared = jnp.dot(shared_rows, shared_up, preferred_element_type=jnp.float32)
    shared_hidden = (jax.nn.silu(gate_shared) * up_shared).astype(jnp.bfloat16)
    shared_hidden = shared_hidden.reshape(tp_count, tok_rows, -1)
    routed_gate = jnp.einsum(
        "qsjcm,jmf->qsjcf", routed, expert_gate, preferred_element_type=jnp.float32
    )
    routed_up = jnp.einsum(
        "qsjcm,jmf->qsjcf", routed, expert_up, preferred_element_type=jnp.float32
    )
    routed_hidden = (jax.nn.silu(routed_gate) * routed_up).astype(jnp.bfloat16)
    block_rows = tok_rows + ep_count * exp_dev * capacity
    group_count = block_rows * lax.axis_size("tp") // block_rows
    shared_out = jnp.einsum(
        "qrf,fm->qrm", shared_hidden, shared_down, preferred_element_type=jnp.float32
    )
    routed_out = jnp.einsum(
        "qsjcf,jfm->qsjcm", routed_hidden, expert_down, preferred_element_type=jnp.float32
    )
    routed_out = routed_out.reshape(group_count, -1, model_width)
    summed = sent_and_summed(
        jnp.concatenate([shared_out, routed_out], axis=1)
        .reshape(block_rows * lax.axis_size("tp"), model_width)
        .astype(jnp.bfloat16),
        "tp",
        0,
    ).astype(jnp.bfloat16)
    shared_result = summed[:tok_rows]
    routed_back = summed[tok_rows:].reshape(ep_count, exp_dev * capacity, model_width)
    returned = two_step_exchange(routed_back, (("ep_0", "ep_1"), "ep_2"), (1, 0), 0, 0).reshape(
        slot_total, model_width
    )
    picked = jnp.take(returned, own_targets, axis=0).reshape(tok_rows, top_k, model_width)
    routed_sum = jnp.sum(route_weights[:, :, None] * picked.astype(jnp.float32), axis=1)
    expert_mix = (shared_result.astype(jnp.float32) + routed_sum).astype(jnp.bfloat16)
    return (mixer_out, expert_mix)


def solution(mesh):
    finer = Mesh(mesh.devices.reshape(4, 4, 2, mesh.shape["tp"]), ("ep_0", "ep_1", "ep_2", "tp"))
    placed = (
        P(EP_TP, None),
        P(EP_TP, None),
        P(EP_TP, None),
        P(),
        P(),
        P(None, "tp"),
        P(None, "tp"),
        P(None, "tp"),
        P("tp", None),
        P(EP_TP, None),
        P(),
        P(EP_TP, None),
        P(EP_TP, None),
        P(None, "tp"),
        P(None, "tp"),
        P("tp", None),
        P(EP, None, "tp"),
        P(EP, None, "tp"),
        P(EP, "tp", None),
    )
    return jax.shard_map(
        on_device,
        mesh=finer,
        in_specs=placed,
        out_specs=(P(EP_TP, None), P(EP_TP, None)),
        check_vma=False,
    )
```

profile of v0, /device:TPU:0, one launch (start us, length us, event | category | flops | bytes accessed | tf_op | source)
XLA Modules:
  0.0 784.0 jit_solution(4837540948085160881)
XLA Ops:
  13.7 3.6 convolution_convert_fusion.12
  17.2 4.6 reshape_reshape_reshape.9
  21.9 4.0 copy.147
  25.9 5.8 all_to_all.25
  34.5 42.3 %all_to_all.26 = bf16[16,2,1,10,4096]{4,1,3,2,0:T(2,128)(2,1)S(1)} all-to-all(bf16[16,2,1,10,4096]{4,1,3,2,0:T(2,128)(2,1)S(1)} %copy.148), channel_id=1, replica_groups=mesh['ep_0'=4,'ep_1'=4,'ep_2'=2,'tp'=4] {'ep_0','ep_1'}, dimensions={0} | all-to-all | bytes 5242880 | tf_op jit(solution)/shard_map/all_to_all | solution.py:41
  76.7 5.0 copy.149
  81.7 5.1 reshape_reshape.3
  87.1 13.9 %all_gather.16 = bf16[512,512]{1,0:T(8,128)(2,1)S(1)} all-gather(bf16[128,512]{1,0:T(8,128)(2,1)S(1)} %fusion.155), channel_id=1, replica_groups=mesh['ep_0'=4,'ep_1'=4,'ep_2'=2,'tp'=4] {'tp'}, dimensions={0}, use_global_device_ids=true | all-gather | bytes 655360 | tf_op jit(solution)/shard_map/all_gather | solution.py:152
  103.9 10.0 %collective-permute-start.2 = (bf16[1024,512]{1,0:T(8,128)(2,1)S(1)}, bf16[1024,512]{1,0:T(8,128)(2,1)S(1)}, u32[]{:S(2)}, u32[]{:S(2)}) collective-permute-start(bf16[1024,512]{1,0:T(8,128)(2,1)S(1)} %pad_maximum_fusion.3), channel_id=1, source_target_pairs={{0,8},{4,12},{8,16},{12,20},{16,24},{20,28},{24,32},{28,36},{32,40... | collective-permute-start | bytes 3145736 | tf_op jit(solution)/shard_map/ppermute | solution.py:22
  113.9 19.8 %collective-permute-done.2 = bf16[1024,512]{1,0:T(8,128)(2,1)S(1)} collective-permute-done((bf16[1024,512]{1,0:T(8,128)(2,1)S(1)}, bf16[1024,512]{1,0:T(8,128)(2,1)S(1)}, u32[]{:S(2)}, u32[]{:S(2)}) %collective-permute-start.2) | collective-permute-done | bytes 1048608 | tf_op jit(solution)/shard_map/ppermute | solution.py:22
  133.9 6.5 collective-permute-start.4
  140.4 43.3 %collective-permute-done.4 = bf16[2048,512]{1,0:T(8,128)(2,1)S(1)} collective-permute-done((bf16[2048,512]{1,0:T(8,128)(2,1)S(1)}, bf16[2048,512]{1,0:T(8,128)(2,1)S(1)}, u32[]{:S(2)}, u32[]{:S(2)}) %collective-permute-start.4) | collective-permute-done | bytes 2097184 | tf_op jit(solution)/shard_map/ppermute | solution.py:22
  187.2 6.1 collective-permute-start.6
  193.2 10.8 %all_gather.17 = bf16[512,64]{0,1:T(8,128)(2,1)S(1)} all-gather(bf16[128,64]{0,1:T(8,128)(2,1)S(1)} %copy-done.30), channel_id=1, replica_groups=mesh['ep_0'=4,'ep_1'=4,'ep_2'=2,'tp'=4] {'tp'}, dimensions={0}, use_global_device_ids=true | all-gather | bytes 81920 | tf_op jit(solution)/shard_map/all_gather | solution.py:153
  204.1 4.3 fusion.180
  211.7 5.3 copy.153
  216.9 60.4 %collective-permute-done.6 = bf16[4096,512]{1,0:T(8,128)(2,1)} collective-permute-done((bf16[4096,512]{1,0:T(8,128)(2,1)}, bf16[4096,512]{1,0:T(8,128)(2,1)}, u32[]{:S(2)}, u32[]{:S(2)}) %collective-permute-start.6) | collective-permute-done | bytes 4194336 | tf_op jit(solution)/shard_map/ppermute | solution.py:22
  277.4 4.5 constant_dynamic-update-slice_fusion.4
  286.0 12.7 %collective-permute-start.8 = (bf16[8192,512]{1,0:T(8,128)(2,1)}, bf16[8192,512]{1,0:T(8,128)(2,1)}, u32[]{:S(2)}, u32[]{:S(2)}) collective-permute-start(bf16[8192,512]{1,0:T(8,128)(2,1)} %constant_dynamic-update-slice_fusion), channel_id=1, source_target_pairs={{0,64},{4,68},{8,72},{12,76},{16,80},{20,84},{24,88},{28,92},{32,9... | collective-permute-start | bytes 25165832 | tf_op jit(solution)/shard_map/ppermute | solution.py:22
  298.7 8.6 %fusion.112 = f32[4,32,1,10,256]{4,1,3,0,2:T(8,128)} fusion(bf16[1,4096,256]{2,1,0:T(8,128)(2,1)} %param.53, bf16[4,32,10,4096]{3,1,0,2:T(8,128)(2,1)} %bitcast.281), kind=kOutput, calls=%fused_computation.131 | convolution fusion | flops 2684354560 | bytes 13893632 | tf_op jit(solution)/shard_map/qsjcm,jmf->qsjcf/dot_general | solution.py:237
  307.4 16.8 %convert_bitcast_fusion = bf16[4,32,1,10,4096]{4,1,3,0,2:T(8,128)(2,1)} fusion(bf16[1,256,4096]{2,1,0:T(8,128)(2,1)S(1)} %copy-done, bf16[1,4096,256]{2,1,0:T(8,128)(2,1)} %param.54, bf16[4,32,10,4096]{3,1,0,2:T(8,128)(2,1)} %bitcast.282, f32[4,32,1,10,256]{4,1,3,0,2:T(8,128)} %fusion.112), kind=kOutput, calls=%fused_computation.101 | convolution fusion | flops 5375918080 | bytes 26476544 | tf_op jit(solution)/shard_map/qsjcf,jfm->qsjcm/dot_general | solution.py:249
  324.2 14.9 %copy.152 = bf16[4,32,1,10,4096]{4,0,3,1,2:T(4,128)(2,1)} copy(bf16[4,32,1,10,4096]{4,1,3,0,2:T(8,128)(2,1)} %convert_bitcast_fusion) | data formatting | bytes 20971520 | tf_op jit(solution)/shard_map/qsjcf,jfm->qsjcm/transpose | solution.py:249
  339.1 18.8 %pad_maximum_fusion = bf16[4,448,4096]{2,0,1:T(4,128)(2,1)S(1)} fusion(bf16[4,320,4096]{2,0,1:T(4,128)(2,1)} %bitcast.268, bf16[4,128,4096]{2,0,1:T(4,128)(2,1)S(1)} %copy-done.15), kind=kLoop, calls=%fused_computation.100 | loop fusion | flops 7340032 | bytes 29360128 | tf_op jit(solution)/shard_map/concatenate | solution.py:254
  357.8 10.0 %copy.154 = bf16[4,448,4096]{2,1,0:T(8,128)(2,1)} copy(bf16[4,448,4096]{2,0,1:T(4,128)(2,1)S(1)} %pad_maximum_fusion) | data formatting | bytes 29360128 | tf_op jit(solution)/shard_map/concatenate | solution.py:254
  367.8 6.8 all-to-all-start.2
  377.2 7.4 collective-permute-start.3
  387.3 7.0 collective-permute-start.5
  396.2 3.4 collective-permute-done.5
  399.6 5.6 collective-permute-start.7
  407.0 88.2 %collective-permute-done.7 = bf16[4096,64]{0,1:T(8,128)(2,1)S(1)} collective-permute-done((bf16[4096,64]{0,1:T(8,128)(2,1)S(1)}, bf16[4096,64]{0,1:T(8,128)(2,1)S(1)}, u32[]{:S(2)}, u32[]{:S(2)}) %collective-permute-start.7) | collective-permute-done | bytes 524320 | tf_op jit(solution)/shard_map/ppermute | solution.py:22
  498.7 6.8 collective-permute-start.9
  509.3 3.2 fusion.171
  513.4 3.0 fusion.101
  519.3 8.3 %collective-permute-done.9 = bf16[8192,64]{0,1:T(8,128)(2,1)} collective-permute-done((bf16[8192,64]{0,1:T(8,128)(2,1)}, bf16[8192,64]{0,1:T(8,128)(2,1)}, u32[]{:S(2)}, u32[]{:S(2)}) %collective-permute-start.9) | collective-permute-done | bytes 1048608 | tf_op jit(solution)/shard_map/ppermute | solution.py:22
  528.8 6.5 convolution_convert_fusion.11
  535.4 7.3 all-to-all-done.2
  542.7 10.7 %reduce_sum.137 = bf16[448,4096]{1,0:T(8,128)(2,1)} reduce(bf16[4,448,4096]{2,1,0:T(8,128)(2,1)} %all-to-all-done.2, bf16[]{:T(256)} %constant.370.clone.1), dimensions={0}, to_apply=%region_38.39 | reduce | flops 5505024 | bytes 18350082 | tf_op jit(solution)/shard_map/reduce_sum | solution.py:54
  555.2 2.8 reshape_reshape_reshape.10
  557.9 3.6 copy.157
  561.6 5.8 all_to_all.27
  567.4 4.2 copy.158
  571.6 137.8 %all-to-all-start.4 = ((bf16[16,2,1,10,4096]{4,1,3,2,0:T(2,128)(2,1)}), bf16[16,2,1,10,4096]{4,1,3,2,0:T(2,128)(2,1)S(1)}, u32[]{:S(2)}, u32[]{:S(2)}) async-start(bf16[16,2,1,10,4096]{4,1,3,2,0:T(2,128)(2,1)} %copy.158), calls=%async_computation.5 | async-start | bytes 5242880 | tf_op jit(solution)/shard_map/all_to_all | solution.py:41
  710.0 40.0 %all-to-all-done.4 = bf16[16,2,1,10,4096]{4,1,3,2,0:T(2,128)(2,1)S(1)} async-done(((bf16[16,2,1,10,4096]{4,1,3,2,0:T(2,128)(2,1)}), bf16[16,2,1,10,4096]{4,1,3,2,0:T(2,128)(2,1)S(1)}, u32[]{:S(2)}, u32[]{:S(2)}) %all-to-all-start.4) | async-done | bytes 2621472 | tf_op jit(solution)/shard_map/all_to_all | solution.py:41
  750.0 4.1 copy.159
  754.1 3.3 reshape_reshape_reshape.11
  757.5 3.2 gather_fusion
  760.6 4.5 gather.7
  765.2 10.9 %multiply_reduce_fusion = f32[128,4096]{1,0:T(8,128)S(1)} fusion(bf16[128,2,4096]{2,1,0:T(2,128)(2,1)} %gather.7, pred[128,2]{1,0:T(8,128)(4,1)S(1)} %copy.156, f32[128,2]{1,0:T(8,128)S(1)} %copy.155), kind=kLoop, calls=%fused_computation.113 | loop fusion | flops 3670016 | bytes 4195584 | tf_op jit(solution)/shard_map/reduce_sum | solution.py:266
  (198 shorter events, 48.1 us)
Async XLA Ops:
  7.2 300.2 %copy-start = (bf16[1,256,4096]{2,1,0:T(8,128)(2,1)S(1)}, bf16[1,256,4096]{2,1,0:T(8,128)(2,1)}, u32[]{:S(2)}) copy-start(bf16[1,256,4096]{2,1,0:T(8,128)(2,1)} %param.55) | copy-start | bytes 6291460
  7.2 4.3 copy-start.33
  7.2 196.9 %all-gather.6.cloned.1.call-start = ((), (), s32[]{:S(2)}) async-start(), calls=%async_computation.8 | async-start | bytes 5242880 | tf_op jit(solution)/shard_map/all_gather | solution.py:229
  11.5 287.3 %all-gather.8.cloned.1.call-start = ((), (), s32[]{:S(2)}) async-start(), calls=%async_computation.9 | async-start | bytes 13107200 | tf_op jit(solution)/shard_map/all_gather | solution.py:230
  12.9 9.0 %copy-start.31 = (s32[256]{0:T(256)}, s32[256]{0:T(256)S(1)}, u32[]{:S(2)}) copy-start(s32[256]{0:T(256)S(1)} %fusion.159) | copy-start | bytes 3076
  81.7 5.2 copy-start.29
  81.7 5.3 copy-start.36
  101.0 86.2 %copy-start.9 = (bf16[512,512]{1,0:T(8,128)(2,1)}, bf16[512,512]{1,0:T(8,128)(2,1)S(1)}, u32[]{:S(2)}) copy-start(bf16[512,512]{1,0:T(8,128)(2,1)S(1)} %all_gather.16) | copy-start | bytes 1572868
  101.0 2.8 collective-permute-start
  103.8 83.3 %copy-start.12 = (bf16[512,512]{1,0:T(8,128)(2,1)}, bf16[512,512]{1,0:T(8,128)(2,1)S(1)}, u32[]{:S(2)}) copy-start(bf16[512,512]{1,0:T(8,128)(2,1)S(1)} %collective-permute-done) | copy-start | bytes 1572868
  103.9 29.8 %collective-permute-start.2 = (bf16[1024,512]{1,0:T(8,128)(2,1)S(1)}, bf16[1024,512]{1,0:T(8,128)(2,1)S(1)}, u32[]{:S(2)}, u32[]{:S(2)}) collective-permute-start(bf16[1024,512]{1,0:T(8,128)(2,1)S(1)} %pad_maximum_fusion.3), channel_id=1, source_target_pairs={{0,8},{4,12},{8,16},{12,20},{16,24},{20,28},{24,32},{28,36},{32,40... | collective-permute-start | bytes 3145736 | tf_op jit(solution)/shard_map/ppermute | solution.py:22
  133.7 149.6 %copy-start.4 = (bf16[1024,512]{1,0:T(8,128)(2,1)}, bf16[1024,512]{1,0:T(8,128)(2,1)S(1)}, u32[]{:S(2)}) copy-start(bf16[1024,512]{1,0:T(8,128)(2,1)S(1)} %collective-permute-done.2) | copy-start | bytes 3145732
  133.9 59.4 %copy-start.30 = (bf16[128,64]{0,1:T(8,128)(2,1)S(1)}, bf16[128,64]{0,1:T(8,128)(2,1)}, u32[]{:S(2)}) copy-start(bf16[128,64]{0,1:T(8,128)(2,1)} %param.39) | copy-start | bytes 49156
  133.9 49.8 %collective-permute-start.4 = (bf16[2048,512]{1,0:T(8,128)(2,1)S(1)}, bf16[2048,512]{1,0:T(8,128)(2,1)S(1)}, u32[]{:S(2)}, u32[]{:S(2)}) collective-permute-start(bf16[2048,512]{1,0:T(8,128)(2,1)S(1)} %pad_maximum_fusion.2), channel_id=1, source_target_pairs={{0,16},{4,20},{8,24},{12,28},{16,32},{20,36},{24,40},{28,44},{32,4... | collective-permute-start | bytes 6291464 | tf_op jit(solution)/shard_map/ppermute | solution.py:22
  187.2 90.2 %collective-permute-start.6 = (bf16[4096,512]{1,0:T(8,128)(2,1)}, bf16[4096,512]{1,0:T(8,128)(2,1)}, u32[]{:S(2)}, u32[]{:S(2)}) collective-permute-start(bf16[4096,512]{1,0:T(8,128)(2,1)} %pad_maximum_fusion.1), channel_id=1, source_target_pairs={{0,32},{4,36},{8,40},{12,44},{16,48},{20,52},{24,56},{28,60},{32,6... | collective-permute-start | bytes 12582920 | tf_op jit(solution)/shard_map/ppermute | solution.py:22
  204.1 4.3 copy-start.39
  204.1 4.7 copy-start.40
  216.9 64.9 %copy-start.7 = (bf16[2048,512]{1,0:T(8,128)(2,1)S(1)}, bf16[2048,512]{1,0:T(8,128)(2,1)}, u32[]{:S(2)}) copy-start(bf16[2048,512]{1,0:T(8,128)(2,1)} %copy-done.6) | copy-start | bytes 6291460
  286.0 241.6 %collective-permute-start.8 = (bf16[8192,512]{1,0:T(8,128)(2,1)}, bf16[8192,512]{1,0:T(8,128)(2,1)}, u32[]{:S(2)}, u32[]{:S(2)}) collective-permute-start(bf16[8192,512]{1,0:T(8,128)(2,1)} %constant_dynamic-update-slice_fusion), channel_id=1, source_target_pairs={{0,64},{4,68},{8,72},{12,76},{16,80},{20,84},{24,88},{28,92},{32,9... | collective-permute-start | bytes 25165832 | tf_op jit(solution)/shard_map/ppermute | solution.py:22
  324.2 14.9 %copy-start.15 = (bf16[4,128,4096]{2,0,1:T(4,128)(2,1)S(1)}, bf16[4,128,4096]{2,0,1:T(4,128)(2,1)}, u32[]{:S(2)}) copy-start(bf16[4,128,4096]{2,0,1:T(4,128)(2,1)} %copy.153) | copy-start | bytes 12582916
  367.8 8.5 %copy-start.28 = (bf16[128,1024]{1,0:T(8,128)(2,1)S(1)}, bf16[128,1024]{1,0:T(8,128)(2,1)}, u32[]{:S(2)}) copy-start(bf16[128,1024]{1,0:T(8,128)(2,1)} %param.37) | copy-start | bytes 786436
  367.8 26.5 %copy-start.35 = (f32[1024]{0:T(1024)S(1)}, f32[1024]{0:T(1024)}, u32[]{:S(2)}) copy-start(f32[1024]{0:T(1024)} %param.40) | copy-start | bytes 12292
  367.8 37.4 %copy-start.2 = (bf16[512,512]{1,0:T(8,128)(2,1)S(1)}, bf16[512,512]{1,0:T(8,128)(2,1)}, u32[]{:S(2)}) copy-start(bf16[512,512]{1,0:T(8,128)(2,1)} %param.43) | copy-start | bytes 1572868
  367.8 37.4 %copy-start.11 = (bf16[512,512]{1,0:T(8,128)(2,1)S(1)}, bf16[512,512]{1,0:T(8,128)(2,1)}, u32[]{:S(2)}) copy-start(bf16[512,512]{1,0:T(8,128)(2,1)} %copy-done.9) | copy-start | bytes 1572868
  367.8 174.9 %all-to-all-start.2 = ((bf16[4,448,4096]{2,1,0:T(8,128)(2,1)}), bf16[4,448,4096]{2,1,0:T(8,128)(2,1)}, u32[]{:S(2)}, u32[]{:S(2)}) async-start(bf16[4,448,4096]{2,1,0:T(8,128)(2,1)} %copy.154), calls=%async_computation.3 | async-start | bytes 29360128 | tf_op jit(solution)/shard_map/all_to_all | solution.py:53
  374.6 31.2 %copy-start.3 = (bf16[512,512]{1,0:T(8,128)(2,1)S(1)}, bf16[512,512]{1,0:T(8,128)(2,1)}, u32[]{:S(2)}) copy-start(bf16[512,512]{1,0:T(8,128)(2,1)} %param.44) | copy-start | bytes 1572868
  374.6 130.9 %all-gather.4.cloned.1.call-start = ((), (), s32[]{:S(2)}) async-start(), calls=%async_computation.6 | async-start | bytes 1310720 | tf_op jit(solution)/shard_map/all_gather | solution.py:151
  375.0 2.2 collective-permute-start.1
  377.2 131.1 %copy-start.20 = (bf16[512,64]{0,1:T(8,128)(2,1)}, bf16[512,64]{0,1:T(8,128)(2,1)S(1)}, u32[]{:S(2)}) copy-start(bf16[512,64]{0,1:T(8,128)(2,1)S(1)} %collective-permute-done.1) | copy-start | bytes 196612
  377.2 10.0 %collective-permute-start.3 = (bf16[1024,64]{0,1:T(8,128)(2,1)S(1)}, bf16[1024,64]{0,1:T(8,128)(2,1)S(1)}, u32[]{:S(2)}, u32[]{:S(2)}) collective-permute-start(bf16[1024,64]{0,1:T(8,128)(2,1)S(1)} %maximum_maximum_fusion.2), channel_id=1, source_target_pairs={{0,8},{4,12},{8,16},{12,20},{16,24},{20,28},{24,32},{28,36},{32,40... | collective-permute-start | bytes 393224 | tf_op jit(solution)/shard_map/ppermute | solution.py:22
  387.3 12.3 %collective-permute-start.5 = (bf16[2048,64]{0,1:T(8,128)(2,1)S(1)}, bf16[2048,64]{0,1:T(8,128)(2,1)S(1)}, u32[]{:S(2)}, u32[]{:S(2)}) collective-permute-start(bf16[2048,64]{0,1:T(8,128)(2,1)S(1)} %maximum_maximum_fusion.1), channel_id=1, source_target_pairs={{0,16},{4,20},{8,24},{12,28},{16,32},{20,36},{24,40},{28,44},{32,4... | collective-permute-start | bytes 786440 | tf_op jit(solution)/shard_map/ppermute | solution.py:22
  395.2 382.1 %reduce-scatter.2.cloned.1.call-start = ((), (), s32[]{:S(2)}) async-start(), calls=%async_computation.7 | async-start | bytes 5242880 | tf_op jit(solution)/shard_map/reduce_scatter | solution.py:210
  399.6 108.7 %copy-start.18 = (bf16[2048,64]{0,1:T(8,128)(2,1)}, bf16[2048,64]{0,1:T(8,128)(2,1)S(1)}, u32[]{:S(2)}) copy-start(bf16[2048,64]{0,1:T(8,128)(2,1)S(1)} %collective-permute-done.5) | copy-start | bytes 786436
  399.6 95.6 %collective-permute-start.7 = (bf16[4096,64]{0,1:T(8,128)(2,1)S(1)}, bf16[4096,64]{0,1:T(8,128)(2,1)S(1)}, u32[]{:S(2)}, u32[]{:S(2)}) collective-permute-start(bf16[4096,64]{0,1:T(8,128)(2,1)S(1)} %maximum_maximum_fusion), channel_id=1, source_target_pairs={{0,32},{4,36},{8,40},{12,44},{16,48},{20,52},{24,56},{28,60},{32,6... | collective-permute-start | bytes 1572872 | tf_op jit(solution)/shard_map/ppermute | solution.py:22
  495.2 14.0 %copy-start.22 = (bf16[4096,64]{0,1:T(8,128)(2,1)}, bf16[4096,64]{0,1:T(8,128)(2,1)S(1)}, u32[]{:S(2)}) copy-start(bf16[4096,64]{0,1:T(8,128)(2,1)S(1)} %collective-permute-done.7) | copy-start | bytes 1572868
  498.7 28.8 %collective-permute-start.9 = (bf16[8192,64]{0,1:T(8,128)(2,1)}, bf16[8192,64]{0,1:T(8,128)(2,1)}, u32[]{:S(2)}, u32[]{:S(2)}) collective-permute-start(bf16[8192,64]{0,1:T(8,128)(2,1)} %constant_dynamic-update-slice_fusion.5), channel_id=1, source_target_pairs={{0,64},{4,68},{8,72},{12,76},{16,80},{20,84},{24,88},{28,92},{32,9... | collective-permute-start | bytes 3145736 | tf_op jit(solution)/shard_map/ppermute | solution.py:22
  508.4 4.1 copy-start.23
  508.4 4.1 copy-start.25
  512.9 3.6 copy-start.8
  513.4 5.0 copy-start.24
  513.4 5.0 copy-start.26
  567.4 142.0 %copy-start.34 = (s32[128,2]{0,1:T(2,128)S(1)}, s32[128,2]{0,1:T(2,128)}, u32[]{:S(2)}) copy-start(s32[128,2]{0,1:T(2,128)} %param.48) | copy-start | bytes 3076
  567.4 142.3 %copy-start.37 = (pred[128,2]{0,1:T(4,128)(4,1)S(1)}, pred[128,2]{0,1:T(4,128)(4,1)}, u32[]{:S(2)}) copy-start(pred[128,2]{0,1:T(4,128)(4,1)} %get-tuple-element.1570) | copy-start | bytes 772
  567.4 142.4 %copy-start.38 = (f32[128,2]{0,1:T(2,128)S(1)}, f32[128,2]{0,1:T(2,128)}, u32[]{:S(2)}) copy-start(f32[128,2]{0,1:T(2,128)} %param.49) | copy-start | bytes 3076
  567.4 142.5 %copy-start.32 = (s32[256]{0:T(256)S(1)}, s32[256]{0:T(256)}, u32[]{:S(2)}) copy-start(s32[256]{0:T(256)} %copy-done.31) | copy-start | bytes 3076
  571.6 178.4 %all-to-all-start.4 = ((bf16[16,2,1,10,4096]{4,1,3,2,0:T(2,128)(2,1)}), bf16[16,2,1,10,4096]{4,1,3,2,0:T(2,128)(2,1)S(1)}, u32[]{:S(2)}, u32[]{:S(2)}) async-start(bf16[16,2,1,10,4096]{4,1,3,2,0:T(2,128)(2,1)} %copy.158), calls=%async_computation.5 | async-start | bytes 5242880 | tf_op jit(solution)/shard_map/all_to_all | solution.py:41
  760.6 16.7 %copy-start.1 = (bf16[1,256,4096]{2,1,0:T(8,128)(2,1)S(1)}, bf16[1,256,4096]{2,1,0:T(8,128)(2,1)}, u32[]{:S(2)}) copy-start(bf16[1,256,4096]{2,1,0:T(8,128)(2,1)} %param.55) | copy-start | bytes 6291460
  765.2 10.9 %copy-start.16 = (bf16[448,4096]{1,0:T(8,128)(2,1)S(1)}, bf16[448,4096]{1,0:T(8,128)(2,1)}, u32[]{:S(2)}) copy-start(bf16[448,4096]{1,0:T(8,128)(2,1)} %reduce_sum.137) | copy-start | bytes 11010052
  (8 other events, 14.3 us)
Sparse Core Ops, SparseCore 0:
  11.6 50.6 all-gather.5
  87.0 98.2 all-gather.7
  395.3 30.1 all-gather.3
  535.5 184.7 reduce-scatter.1
where the time goes:
time: 798 us; the launch traced here: 784 us
  waiting for transfers between devices  276 us (35%)
  starting transfers between devices  210 us (26%)
  local copies, waits for them, and re-layouts  95.1 us (12%)
  blocking collectives  78.6 us (10%)
  other arithmetic  55.7 us (7%)
  matrix products  52.7 us (7%)
  between operations  14.7 us (2%)
    ppermute x10, waiting for transfers between devices, passed_along(): lax.ppermute(value, axis, [(source, source + steps) for source in range(i...  228 us
    all_to_all x1, starting transfers between devices, turned_blocks(): out = lax.all_to_all(out, axes[k], k, k, tiled=True)  138 us
    ppermute x10, starting transfers between devices, passed_along(): lax.ppermute(value, axis, [(source, source + steps) for source in range(i...  64.8 us
    all_to_all x3, blocking collectives, turned_blocks(): out = lax.all_to_all(out, axes[k], k, k, tiled=True)  53.9 us
    all_to_all x1, waiting for transfers between devices, turned_blocks(): out = lax.all_to_all(out, axes[k], k, k, tiled=True)  40 us
    concatenate x1, other arithmetic, on_device(): jnp.concatenate([shared_out, routed_out], axis=1)  18.8 us
    dot_general x1, matrix products, on_device(): jnp.einsum('qsjcf,jfm->qsjcm', routed_hidden, expert_down, preferred_elem...  16.8 us
    all_to_all x4, local copies, waits for them, and re-layouts, turned_blocks(): out = lax.all_to_all(out, axes[k], k, k, tiled=True)  16 us
  transfers between devices with their start and end apart: 16, of which 11 were waited for; matrix products, arithmetic and copies ran while one was open for 25% of the time, Pallas kernels for 0%

commit v1 on v0

v1 whole, which is shorter than its diff:
```python
import functools

import jax
import jax.numpy as jnp
import numpy as np
from jax import lax
from jax.experimental import pallas as pl
from jax.experimental.pallas import tpu as pltpu
from jax.sharding import Mesh
from jax.sharding import PartitionSpec as P

NOPE = 128
ROPE = 64
VDIM = 128
HEADS_DEV = 4
EP = ("ep_0", "ep_1", "ep_2")
EP_TP = ("ep_0", "ep_1", "ep_2", "tp")
N_EP = 32
N_TP = 4
ROWS = 128
GROUP = 512
WIDTH = 4096
CAP = 10
CHUNKS = 4
CHUNK = WIDTH // CHUNKS
WIRE = CAP * CHUNKS
SLOTS = N_EP * CAP
HALF = SLOTS // 2
PACKED = GROUP + ROPE
CALLS = 4
FORWARD_AFTER = 2

epsilon = 1e-06
rope_theta = 10000.0
bf16 = jnp.bfloat16
f32 = jnp.float32
i32 = jnp.int32


def whole(shape, dtype=bf16):
    return jax.ShapeDtypeStruct(shape, dtype)


def kernel_call(body, out_shape, flops=1000000, **kw):
    return pl.pallas_call(
        body,
        out_shape=out_shape,
        cost_estimate=pl.CostEstimate(flops=int(flops), bytes_accessed=1000000, transcendentals=0),
        **kw,
    )


def ring(steps):
    return [(i, (i + steps) % N_TP) for i in range(N_TP)]


def up(x):
    return lax.ppermute(x, "tp", ring(1))


def down(x):
    return lax.ppermute(x, "tp", ring(N_TP - 1))


def after(x, *deps):
    return lax.optimization_barrier((x, deps))[0]


def rope_angles(positions, rope_width):
    frequency = rope_theta ** (-jnp.arange(0, rope_width, 2, dtype=f32) / rope_width)
    angles = positions.astype(f32)[:, None] * frequency[None, :]
    return (jnp.cos(angles), jnp.sin(angles))


def rotate_pairs(values, cos_tab, sin_tab):
    half_width = values.shape[-1] // 2
    a = values[..., :half_width]
    b = values[..., half_width:]
    return jnp.concatenate([a * cos_tab - b * sin_tab, b * cos_tab + a * sin_tab], axis=-1)


def regroup_matrix():
    out = np.zeros((8 * WIRE, 8 * WIRE), np.float32)
    for c in range(CHUNKS):
        for s in range(8):
            for k in range(CAP):
                out[c * 8 * CAP + s * CAP + k, s * WIRE + c * CAP + k] = 1
    return out


def dispatch_body(tok_ref, gain_ref, routes_ref, norm_ref, wire_ref):
    x = tok_ref[...].astype(f32)
    mean = jnp.mean(x * x, axis=-1, keepdims=True)
    normed = ((x * lax.rsqrt(mean + epsilon)) * gain_ref[...]).astype(bf16)
    norm_ref[...] = normed
    r0 = routes_ref[0:1, :]
    r1 = routes_ref[1:2, :]
    expert = lax.broadcasted_iota(i32, (N_EP, ROWS), 0)
    hot0 = jnp.where(expert == r0, 1.0, 0.0)
    hot1 = jnp.where(expert == r1, 1.0, 0.0)
    before = lax.broadcasted_iota(i32, (ROWS, ROWS), 0) < lax.broadcasted_iota(i32, (ROWS, ROWS), 1)
    before = jnp.where(before, 1.0, 0.0).astype(bf16)
    seen0 = jnp.dot(hot0.astype(bf16), before, preferred_element_type=f32)
    seen1 = jnp.dot(hot1.astype(bf16), before, preferred_element_type=f32)
    seen1 = seen1 + jnp.sum(hot0, axis=1, keepdims=True)
    slot0 = jnp.sum(seen0 * hot0, axis=0, keepdims=True).astype(i32) + r0 * WIRE
    slot1 = jnp.sum(seen1 * hot1, axis=0, keepdims=True).astype(i32) + r1 * WIRE
    row = lax.broadcasted_iota(i32, (N_EP * WIRE, ROWS), 0)
    picks = jnp.concatenate(
        [
            jnp.where((row == slot0 + c * CAP) | (row == slot1 + c * CAP), 1.0, 0.0).astype(bf16)
            for c in range(CHUNKS)
        ],
        axis=1,
    )
    stacked = jnp.concatenate([normed[:, c * CHUNK : (c + 1) * CHUNK] for c in range(CHUNKS)], axis=0)
    wire_ref[...] = jnp.dot(picks, stacked, preferred_element_type=f32).astype(bf16)


def unwire_body(wire_ref, mat_ref, lo_ref, hi_ref):
    mat = mat_ref[...]
    for g in range(4):
        got = jnp.dot(mat, wire_ref[g * 8 * WIRE : (g + 1) * 8 * WIRE, :], preferred_element_type=f32)
        got = got.astype(bf16)
        out_ref = lo_ref if g < 2 else hi_ref
        base = (g % 2) * 8 * CAP
        for c in range(CHUNKS):
            out_ref[base : base + 8 * CAP, c * CHUNK : (c + 1) * CHUNK] = got[c * 8 * CAP : (c + 1) * 8 * CAP, :]


def rewire_body(ol, oh, ml, mh, pl_, ph, mat_ref, wire_ref):
    mat = mat_ref[...]
    for g in range(4):
        own, fm, fp = (ol, ml, pl_) if g < 2 else (oh, mh, ph)
        base = (g % 2) * 8 * CAP
        pieces = []
        for c in range(CHUNKS):
            sl = (slice(base, base + 8 * CAP), slice(c * CHUNK, (c + 1) * CHUNK))
            total = own[sl].astype(f32) + fm[sl].astype(f32) + fp[sl].astype(f32)
            pieces.append(total.astype(bf16))
        rows = jnp.concatenate(pieces, axis=0)
        got = jnp.dot(mat, rows, preferred_element_type=f32)
        wire_ref[g * 8 * WIRE : (g + 1) * 8 * WIRE, :] = got.astype(bf16)


def ffn_body(*refs):
    count = (len(refs) - 3) // 2
    xs, (gate, upw, downw), outs = refs[:count], refs[count : count + 3], refs[count + 3 :]
    for x_ref, out_ref in zip(xs, outs):
        x = x_ref[...]
        g = jnp.dot(x, gate[...], preferred_element_type=f32)
        u = jnp.dot(x, upw[...], preferred_element_type=f32)
        hidden = ((g / (1.0 + jnp.exp(-g))) * u).astype(bf16)
        out_ref[...] = jnp.dot(hidden, downw[...], preferred_element_type=f32).astype(bf16)


def ffn(xs, gate, upw, downw):
    rows = sum(x.shape[0] for x in xs)
    call = kernel_call(ffn_body, tuple(whole(x.shape) for x in xs), flops=rows * WIDTH * 256 * 6)
    return call(*xs, gate, upw, downw)


def combine_body(ret_ref, routes_ref, rw_ref, own, ml, mh, pl_, ph, out_ref):
    r0 = routes_ref[:, 0:1]
    r1 = routes_ref[:, 1:2]
    expert = lax.broadcasted_iota(i32, (ROWS, N_EP), 1)
    hot0 = jnp.where(expert == r0, 1.0, 0.0)
    hot1 = jnp.where(expert == r1, 1.0, 0.0)
    before = lax.broadcasted_iota(i32, (ROWS, ROWS), 1) < lax.broadcasted_iota(i32, (ROWS, ROWS), 0)
    before = jnp.where(before, 1.0, 0.0).astype(bf16)
    seen0 = jnp.dot(before, hot0.astype(bf16), preferred_element_type=f32)
    seen1 = jnp.dot(before, hot1.astype(bf16), preferred_element_type=f32)
    seen1 = seen1 + jnp.sum(hot0, axis=0, keepdims=True)
    slot0 = jnp.sum(seen0 * hot0, axis=1, keepdims=True).astype(i32) + r0 * WIRE
    slot1 = jnp.sum(seen1 * hot1, axis=1, keepdims=True).astype(i32) + r1 * WIRE
    col = lax.broadcasted_iota(i32, (ROWS, N_EP * WIRE), 1)
    w0 = rw_ref[:, 0:1]
    w1 = rw_ref[:, 1:2]
    ret = ret_ref[...]
    for c in range(CHUNKS):
        picks = jnp.concatenate(
            [
                jnp.where(col == slot0 + c * CAP, 1.0, 0.0).astype(bf16),
                jnp.where(col == slot1 + c * CAP, 1.0, 0.0).astype(bf16),
            ],
            axis=0,
        )
        got = jnp.dot(picks, ret, preferred_element_type=f32)
        routed = w0 * got[:ROWS] + w1 * got[ROWS:]
        cols = slice(c * CHUNK, (c + 1) * CHUNK)
        for h, fm, fp in ((0, ml, pl_), (1, mh, ph)):
            rows = slice(h * 64, h * 64 + 64)
            shared = own[rows, cols].astype(f32) + fm[:, cols].astype(f32) + fp[:, cols].astype(f32)
            shared = shared.astype(bf16).astype(f32)
            out_ref[rows, cols] = (shared + routed[h * 64 : h * 64 + 64]).astype(bf16)


def prep_body(q_ref, kv_ref, rot_ref, gq_ref, gkv_ref, out_ref):
    def norm(ref, gain):
        x = ref[...].astype(f32)
        mean = jnp.mean(x * x, axis=-1, keepdims=True)
        return ((x * lax.rsqrt(mean + epsilon)) * gain[...]).astype(bf16)

    out_ref[0:ROWS, :] = norm(q_ref, gq_ref)
    kv = norm(kv_ref, gkv_ref)
    out_ref[ROWS : ROWS + 64, 0:512] = kv[:64]
    out_ref[ROWS : ROWS + 64, 512:1024] = kv[64:]
    out_ref[ROWS + 64 : ROWS + 72, :] = rot_ref[...]


def attend_body(first, last, base, blocks, rank_ref, q_ref, lat_ref, wk_ref, wv_ref, *refs):
    if first:
        state_in = None
    else:
        state_in, refs = refs[:3], refs[3:]
    if last:
        out_ref, refs = refs[0], refs[1:]
        kcat, val, m_ref, l_ref, acc_ref = refs
    else:
        m_out, l_out, acc_out = refs[:3]
        kcat, val, m_ref, l_ref, acc_ref = refs[3:]
    step = pl.program_id(0)
    rank = rank_ref[0]
    block = step + base

    @pl.when(step == 0)
    def _():
        if first:
            m_ref[...] = jnp.full(m_ref.shape, -jnp.inf, f32)
            l_ref[...] = jnp.zeros(l_ref.shape, f32)
            acc_ref[...] = jnp.zeros(acc_ref.shape, f32)
        else:
            m_ref[...] = state_in[0][...]
            l_ref[...] = state_in[1][...]
            acc_ref[...] = state_in[2][...]

    def work(diagonal):
        kv = lat_ref[0:GROUP, :]
        keys = jnp.dot(kv, wk_ref[...], preferred_element_type=f32).astype(bf16)
        val[...] = jnp.dot(kv, wv_ref[...], preferred_element_type=f32).astype(bf16)
        low = lax.broadcasted_iota(i32, (ROPE, 128), 1) < ROPE
        zero = jnp.zeros((ROPE, 128), bf16)
        rots = []
        for i in range(4):
            pair = lat_ref[GROUP : GROUP + ROPE, i * 128 : (i + 1) * 128]
            rots += [jnp.where(low, pair, zero), jnp.where(low, zero, pair)]
        rot = jnp.concatenate(rots, axis=0)
        for h in range(HEADS_DEV):
            kcat[:, h * 256 : h * 256 + 128] = keys[:, h * 128 : (h + 1) * 128]
            kcat[:, h * 256 + 128 : (h + 1) * 256] = rot
        scale = (NOPE + ROPE) ** (-0.5) * 1.4426950408889634

        def score(h):
            return lax.dot_general(
                q_ref[:, h * 256 : (h + 1) * 256],
                kcat[:, h * 256 : (h + 1) * 256],
                (((1,), (1,)), ((), ())),
                preferred_element_type=f32,
            )

        ahead = score(0)
        for h in range(HEADS_DEV):
            scores = ahead
            if h + 1 < HEADS_DEV:
                ahead = score(h + 1)
            if diagonal:
                row_id = lax.broadcasted_iota(i32, (GROUP, GROUP), 0)
                col_id = lax.broadcasted_iota(i32, (GROUP, GROUP), 1)
                scores = jnp.where(row_id >= col_id, scores, -jnp.inf)
            m_old = m_ref[h]
            m_new = jnp.maximum(m_old, jnp.max(scores, axis=-1, keepdims=True))
            factor = jnp.exp2((m_old - m_new) * scale)
            wide = jnp.concatenate([m_new] * 4, axis=1)
            terms = jnp.exp2((scores - wide) * scale)
            part = (terms[:, 0:128] + terms[:, 128:256]) + (terms[:, 256:384] + terms[:, 384:512])
            m_ref[h] = m_new
            l_ref[h] = l_ref[h] * factor + part
            update = jnp.dot(
                terms.astype(bf16), val[:, h * 128 : (h + 1) * 128], preferred_element_type=f32
            )
            acc_ref[h] = acc_ref[h] * factor + update

    @pl.when(block < rank)
    def _():
        work(False)

    @pl.when(block == rank)
    def _():
        work(True)

    @pl.when(step == blocks - 1)
    def _():
        if last:
            for h in range(HEADS_DEV):
                total = jnp.sum(l_ref[h], axis=-1, keepdims=True)
                out_ref[:, h * 128 : (h + 1) * 128] = (acc_ref[h] / total).astype(bf16)
        else:
            m_out[...] = m_ref[...]
            l_out[...] = l_ref[...]
            acc_out[...] = acc_ref[...]


def attend(call_num, rank, q, latents, w_key, w_value, state):
    blocks = N_EP // CALLS
    base = call_num * blocks
    first = call_num == 0
    last = call_num == CALLS - 1
    state_shape = (HEADS_DEV, GROUP, 128)
    same2 = lambda i, r: (0, 0)
    same3 = lambda i, r: (0, 0, 0)
    in_specs = [
        pl.BlockSpec((GROUP, HEADS_DEV * 256), same2),
        pl.BlockSpec((PACKED, GROUP), lambda i, r: (jnp.minimum(i + base, r[0]), 0)),
        pl.BlockSpec((512, 512), same2),
        pl.BlockSpec((512, 512), same2),
    ]
    args = [q, latents, w_key, w_value]
    if not first:
        in_specs += [pl.BlockSpec(state_shape, same3)] * 3
        args += list(state)
    if last:
        out_shape = whole((GROUP, HEADS_DEV * VDIM))
        out_specs = pl.BlockSpec((GROUP, HEADS_DEV * VDIM), same2)
    else:
        out_shape = (whole(state_shape, f32),) * 3
        out_specs = (pl.BlockSpec(state_shape, same3),) * 3
    return pl.pallas_call(
        functools.partial(attend_body, first, last, base, blocks),
        out_shape=out_shape,
        grid_spec=pltpu.PrefetchScalarGridSpec(
            num_scalar_prefetch=1,
            grid=(blocks,),
            in_specs=in_specs,
            out_specs=out_specs,
            scratch_shapes=[
                pltpu.VMEM((GROUP, HEADS_DEV * 256), bf16),
                pltpu.VMEM((GROUP, HEADS_DEV * VDIM), bf16),
                pltpu.VMEM(state_shape, f32),
                pltpu.VMEM(state_shape, f32),
                pltpu.VMEM(state_shape, f32),
            ],
        ),
        compiler_params=pltpu.CompilerParams(dimension_semantics=("arbitrary",)),
        cost_estimate=pl.CostEstimate(
            flops=int(blocks * 1.4e9), bytes_accessed=10000000, transcendentals=0
        ),
    )(rank, *args)


def on_device(
    q_latent,
    kv_latent,
    rope_key,
    gain_query,
    gain_latent,
    w_query,
    w_key,
    w_value,
    w_out,
    tokens_b,
    gain_norm,
    routes,
    route_weights,
    shared_gate,
    shared_up,
    shared_down,
    expert_gate,
    expert_up,
    expert_down,
):
    rank = lax.axis_index(EP)
    tp_rank = lax.axis_index("tp")
    regroup = jnp.asarray(regroup_matrix(), bf16)
    regroup_back = jnp.asarray(regroup_matrix().T, bf16)
    expert_gate, expert_up, expert_down = expert_gate[0], expert_up[0], expert_down[0]

    normed, wire = kernel_call(
        dispatch_body, (whole((ROWS, WIDTH)), whole((N_EP * WIRE, CHUNK))), flops=2e9
    )(tokens_b, gain_norm.reshape(1, WIDTH), routes.T)
    s_lo, s_hi = normed[:64], normed[64:]
    sm_lo, sp_hi = up(s_lo), down(s_hi)
    sm_hi, sp_lo = up(s_hi), down(s_lo)
    arrived = lax.all_to_all(wire.reshape(N_EP, WIRE, CHUNK), EP, 0, 0, tiled=True)
    x_lo, x_hi = kernel_call(unwire_body, (whole((HALF, WIDTH)),) * 2, flops=2e9)(
        arrived.reshape(N_EP * WIRE, CHUNK), regroup
    )

    positions = rank * GROUP + jnp.arange(GROUP, dtype=i32)
    cos_tab, sin_tab = rope_angles(positions, ROPE)
    own_cos, own_sin = rope_angles(
        rank * GROUP + tp_rank * ROWS + jnp.arange(ROWS, dtype=i32), ROPE
    )
    rot_key = rotate_pairs(rope_key.astype(f32), own_cos, own_sin).astype(bf16)
    rot_pair = jnp.concatenate([rot_key[:64], rot_key[64:]], axis=1)
    rot_rows = jnp.concatenate([rot_pair[8 * g : 8 * g + 8] for g in range(8)], axis=1)
    pack = kernel_call(prep_body, whole((200, 1024)), flops=1e6)(
        q_latent, kv_latent, rot_rows, gain_query.reshape(1, -1), gain_latent.reshape(1, -1)
    )
    packs = lax.all_gather(pack, "tp", axis=0, tiled=False)
    kv_part = packs[:, ROWS : ROWS + 64]
    kv_rows = jnp.concatenate(
        [kv_part[t, :, h * 512 : (h + 1) * 512] for t in range(N_TP) for h in range(2)], axis=0
    )
    rot_part = packs[:, ROWS + 64 :]
    rot_rows = jnp.concatenate(
        [
            jnp.concatenate([rot_part[t, :, g * 128 : (g + 1) * 128] for g in range(8)], axis=0)
            for t in range(N_TP)
        ],
        axis=1,
    )
    latents = jnp.concatenate([kv_rows, rot_rows], axis=0)
    latents = lax.all_gather(latents, EP, axis=0, tiled=True)

    s2_lo, s2_hi = up(sm_lo), down(sp_hi)
    m_lo, p_hi = up(x_lo), down(x_hi)
    m_hi, p_lo = up(x_hi), down(x_lo)
    t_lo, t_hi = up(m_lo), down(p_hi)

    shared_w = (shared_gate, shared_up, shared_down)
    routed_w = (expert_gate, expert_up, expert_down)
    (own_s,) = ffn((after(normed, x_lo),), *shared_w)

    query_in = after(packs[:, :ROWS].reshape(GROUP, 1024), own_s)
    query_full = jnp.dot(query_in, w_query, preferred_element_type=f32)
    query_full = query_full.reshape(GROUP, HEADS_DEV, NOPE + ROPE)
    query_rot = rotate_pairs(
        query_full[:, :, NOPE:], cos_tab[:, None, :], sin_tab[:, None, :]
    ).astype(bf16)
    query_nope = query_full[:, :, :NOPE].astype(bf16)
    queries = jnp.concatenate([query_nope, query_rot, query_rot], axis=-1).reshape(GROUP, -1)

    own_lo, own_hi = ffn((after(x_lo, queries), x_hi), *routed_w)
    ms_lo, ms_hi, ps_lo, ps_hi = ffn((after(sm_lo, own_lo), sm_hi, sp_lo, sp_hi), *shared_w)
    ts_lo, ts_hi = ffn((after(s2_lo, ms_lo), s2_hi), *shared_w)
    mr_lo, mr_hi, pr_lo, pr_hi = ffn((after(m_lo, ts_lo), m_hi, p_lo, p_hi), *routed_w)
    tr_lo, tr_hi = ffn((after(t_lo, mr_lo), t_hi), *routed_w)

    def add(a, b):
        return (a.astype(f32) + b.astype(f32)).astype(bf16)

    fm_hi, fp_lo = up(pr_hi), down(mr_lo)
    via_lo, via_hi = up(tr_lo), down(tr_hi)
    svia_lo, svia_hi = up(ts_lo), down(ts_hi)
    sfm_hi, sfp_lo = up(ps_hi), down(ms_lo)

    rank_arr = jnp.full((1,), rank, i32)
    state = None
    states = []
    queries = after(queries, tr_lo)
    for call_num in range(CALLS):
        state = attend(call_num, rank_arr, queries, latents, w_key, w_value, state)
        states.append(state)

    ready = states[FORWARD_AFTER][1]
    via_lo, via_hi, svia_lo, svia_hi = lax.optimization_barrier(
        ((via_lo, via_hi, svia_lo, svia_hi), ready)
    )[0]
    fm_lo, fp_hi = up(add(pr_lo, via_lo)), down(add(mr_hi, via_hi))
    sfm_lo, sfp_hi = up(add(ps_lo, svia_lo)), down(add(ms_hi, svia_hi))

    back = kernel_call(rewire_body, whole((N_EP * WIRE, CHUNK)), flops=2e9)(
        own_lo, own_hi, fm_lo, fm_hi, fp_lo, fp_hi, regroup_back
    )
    returned = lax.all_to_all(back.reshape(N_EP, WIRE, CHUNK), EP, 0, 0, tiled=True)

    partial = jnp.dot(state, w_out, preferred_element_type=f32).astype(bf16)
    mixer_out = lax.psum_scatter(partial, "tp", scatter_dimension=0, tiled=True)

    expert_mix = kernel_call(combine_body, whole((ROWS, WIDTH)), flops=3e9)(
        returned.reshape(N_EP * WIRE, CHUNK),
        routes,
        route_weights,
        own_s,
        sfm_lo,
        sfm_hi,
        sfp_lo,
        sfp_hi,
    )
    return (mixer_out, expert_mix)


def solution(mesh):
    finer = Mesh(mesh.devices.reshape(4, 4, 2, mesh.shape["tp"]), ("ep_0", "ep_1", "ep_2", "tp"))
    placed = (
        P(EP_TP, None),
        P(EP_TP, None),
        P(EP_TP, None),
        P(),
        P(),
        P(None, "tp"),
        P(None, "tp"),
        P(None, "tp"),
        P("tp", None),
        P(EP_TP, None),
        P(),
        P(EP_TP, None),
        P(EP_TP, None),
        P(None, "tp"),
        P(None, "tp"),
        P("tp", None),
        P(EP, None, "tp"),
        P(EP, None, "tp"),
        P(EP, "tp", None),
    )
    return jax.shard_map(
        on_device,
        mesh=finer,
        in_specs=placed,
        out_specs=(P(EP_TP, None), P(EP_TP, None)),
        check_vma=False,
    )
```

time: 798 us -> 558 us (0.70)
  starting transfers between devices: 210 us -> 116 us
  Pallas kernels: 0 us -> 92.2 us
  blocking collectives: 78.6 us -> 0 us
  local copies, waits for them, and re-layouts: 95.1 us -> 22.7 us
  other arithmetic: 55.7 us -> 2.01 us
  matrix products: 52.7 us -> 9.08 us
  waiting for transfers between devices: 276 us -> 292 us
    pallas_call x0 -> x15, Pallas kernels: none -> 92.2 us  [the longest x6 45.9 us: ffn(): return call(*xs, gate, upw, downw)]
    all_to_all x2, starting transfers between devices: 145 us -> 81.1 us  [the longest x1 73.5 us: on_device(): lax.all_to_all(back.reshape(N_EP, WIRE, CHUNK), EP, 0, 0, tiled=True)]
    all_to_all x3 -> x0, blocking collectives: 53.9 us -> none  [turned_blocks(): out = lax.all_to_all(out, axes[k], k, k, tiled=True)]
    dot_general x13 -> x2, matrix products: 52.7 us -> 9.08 us  [the longest x1 6.69 us: on_device(): partial = jnp.dot(state, w_out, preferred_element_type=f32).astype(bf16)]
    ppermute x10 -> x24, starting transfers between devices: 64.8 us -> 34.9 us  [the longest x12 26.8 us: down(): return lax.ppermute(x, 'tp', ring(N_TP - 1))]
    all_gather x3 -> x2, waiting for transfers between devices: 0.04 us -> 29.6 us  [the longest x1 29.6 us: on_device(): packs = lax.all_gather(pack, 'tp', axis=0, tiled=False)]
    another operation x8 -> x0, local copies, waits for them, and re-layouts: 28.8 us -> none  [the longest x4 15 us: turned_blocks(): out = pieces.reshape(*(lax.axis_size(a) for a in axes), *inside)]
    reduce_sum x7 -> x0, other arithmetic: 26.7 us -> none  [the longest x1 10.9 us: on_device(): jnp.sum(route_weights[:, :, None] * picked.astype(jnp.float32), axis=1)]
  transfers between devices with their start and end apart: 16 -> 29, of which waited for: 11 -> 14; matrix products, arithmetic and copies ran while one was open for 25% -> 2% of each run, Pallas kernels for 0% -> 13%
where the time goes in v1:
time: 558 us; the launch traced here: 548 us
  waiting for transfers between devices  292 us (52%)
  starting transfers between devices  116 us (21%)
  Pallas kernels  92.2 us (17%)
  local copies, waits for them, and re-layouts  22.7 us (4%)
  between operations  14.3 us (3%)
  matrix products  9.08 us (2%)
    ppermute x12, waiting for transfers between devices, down(): return lax.ppermute(x, 'tp', ring(N_TP - 1))  136 us
    ppermute x12, waiting for transfers between devices, up(): return lax.ppermute(x, 'tp', ring(1))  78.9 us
    all_to_all x1, starting transfers between devices, on_device(): lax.all_to_all(back.reshape(N_EP, WIRE, CHUNK), EP, 0, 0, tiled=True)  73.5 us
    pallas_call x6, Pallas kernels, ffn(): return call(*xs, gate, upw, downw)  45.9 us
    all_to_all x1, waiting for transfers between devices, on_device(): lax.all_to_all(wire.reshape(N_EP, WIRE, CHUNK), EP, 0, 0, tiled=True)  41.1 us
    all_gather x1, waiting for transfers between devices, on_device(): packs = lax.all_gather(pack, 'tp', axis=0, tiled=False)  29.6 us
    ppermute x12, starting transfers between devices, down(): return lax.ppermute(x, 'tp', ring(N_TP - 1))  26.8 us
    pallas_call x4, Pallas kernels, attend(): pl.pallas_call(functools.partial(attend_body, first, last, base, blocks),...  21.4 us
  transfers between devices with their start and end apart: 29, of which 14 were waited for; matrix products, arithmetic and copies ran while one was open for 2% of the time, Pallas kernels for 13%

profile of v1, /device:TPU:0, one launch (start us, length us, event | category | flops | bytes accessed | tf_op | source)
XLA Modules:
  0.0 548.0 jit_solution(11920665160059417240)
XLA Ops:
  9.4 2.0 shard_map.212
  11.5 29.6 %all-gather.6.cloned.1.call-done = bf16[800,1024]{1,0:T(8,128)(2,1)} async-done(((bf16[200,1024]{1,0:T(8,128)(2,1)}), bf16[800,1024]{1,0:T(8,128)(2,1)}) %all-gather.6.cloned.1.call-update) | async-done | bytes 1638416 | tf_op jit(solution)/shard_map/all_gather | solution.py:399
  54.2 4.7 shard_map.213
  59.0 7.5 %all-to-all-start = ((bf16[32,40,1024]{2,1,0:T(8,128)(2,1)}), bf16[32,40,1024]{2,1,0:T(8,128)(2,1)}, u32[]{:S(2)}, u32[]{:S(2)}) async-start(bf16[32,40,1024]{2,1,0:T(8,128)(2,1)} %bitcast.190), calls=%async_computation | async-start | bytes 5242880 | tf_op jit(solution)/shard_map/all_to_all | solution.py:383
  68.0 41.1 %all-to-all-done = bf16[32,40,1024]{2,1,0:T(8,128)(2,1)} async-done(((bf16[32,40,1024]{2,1,0:T(8,128)(2,1)}), bf16[32,40,1024]{2,1,0:T(8,128)(2,1)}, u32[]{:S(2)}, u32[]{:S(2)}) %all-to-all-start) | async-done | bytes 2621472 | tf_op jit(solution)/shard_map/all_to_all | solution.py:383
  109.1 4.5 shard_map.214
  113.7 1.3 collective-permute-start
  115.0 1.9 collective-permute-start.10
  116.9 1.3 collective-permute-start.6
  118.9 2.6 collective-permute-start.5
  122.9 5.5 %shard_map.215.own = bf16[128,4096]{1,0:T(8,128)(2,1)} custom-call(bf16[128,4096]{1,0:T(8,128)(2,1)} %get-tuple-element.44.refs_0_, bf16[4096,256]{1,0:T(8,128)(2,1)} %refs_2_.3, bf16[4096,256]{1,0:T(8,128)(2,1)} %refs_3_.3, bf16[256,4096]{1,0:T(8,128)(2,1)} %refs_4_.3), custom_call_target="tpu_custom_call" | custom-call | flops 805306368 | bytes 1000000 | tf_op jit(solution)/shard_map/pallas_call | solution.py:160
  128.4 2.4 fusion.12
  130.8 27.4 %collective-permute-done.6.refs_3_ = bf16[64,4096]{1,0:T(8,128)(2,1)} collective-permute-done((bf16[64,4096]{1,0:T(8,128)(2,1)}, bf16[64,4096]{1,0:T(8,128)(2,1)}, u32[]{:S(2)}, u32[]{:S(2)}) %collective-permute-start.6) | collective-permute-done | bytes 524320 | tf_op jit(solution)/shard_map/ppermute | solution.py:62
  158.2 1.5 collective-permute-start.3
  159.7 1.7 collective-permute-start.9
  161.4 8.0 %collective-permute-done.5.refs_2_ = bf16[64,4096]{1,0:T(8,128)(2,1)} collective-permute-done((bf16[64,4096]{1,0:T(8,128)(2,1)}, bf16[64,4096]{1,0:T(8,128)(2,1)}, u32[]{:S(2)}, u32[]{:S(2)}) %collective-permute-start.5) | collective-permute-done | bytes 524320 | tf_op jit(solution)/shard_map/ppermute | solution.py:62
  169.4 1.5 collective-permute-start.8
  172.2 2.1 collective-permute-start.11
  175.1 1.5 copy.38.q_ref
  176.6 7.2 %shard_map.216 = (bf16[160,4096]{1,0:T(8,128)(2,1)}, bf16[160,4096]{1,0:T(8,128)(2,1)}) custom-call(bf16[160,4096]{1,0:T(8,128)(2,1)} %get-tuple-element.46.refs_0_, bf16[160,4096]{1,0:T(8,128)(2,1)} %get-tuple-element.47.refs_1_, bf16[4096,256]{1,0:T(8,128)(2,1)} %bitcast.181, bf16[4096,256]{1,0:T(8,128)(2,1)} %bitcast.184, bf16[256,4096]{1,0:T(8,128)(2,1)} %bitcast.187), custom_call_target="tpu_custom_call" | custom-call | flops 2013265920 | bytes 1000000 | tf_op jit(solution)/shard_map/pallas_call | solution.py:160
  183.8 9.1 %shard_map.217 = (bf16[64,4096]{1,0:T(8,128)(2,1)}, bf16[64,4096]{1,0:T(8,128)(2,1)}, bf16[64,4096]{1,0:T(8,128)(2,1)}, bf16[64,4096]{1,0:T(8,128)(2,1)}) custom-call(bf16[64,4096]{1,0:T(8,128)(2,1)} %collective-permute-done.2.refs_0_, bf16[64,4096]{1,0:T(8,128)(2,1)} %collective-permute-done.4.refs_1_, bf16[64,4096]{1,0:T(8,128)(2,1)} %collective-permute-done.5.refs_2_, ...), custom_call_target="tpu_custom_call" | custom-call | flops 1610612736 | bytes 1000000 | tf_op jit(solution)/shard_map/pallas_call | solution.py:160
  192.9 41.0 %collective-permute-done.7.refs_1_ = bf16[64,4096]{1,0:T(8,128)(2,1)S(1)} collective-permute-done((bf16[64,4096]{1,0:T(8,128)(2,1)}, bf16[64,4096]{1,0:T(8,128)(2,1)S(1)}, u32[]{:S(2)}, u32[]{:S(2)}) %collective-permute-start.7) | collective-permute-done | bytes 524320 | tf_op jit(solution)/shard_map/ppermute | solution.py:62
  234.7 6.4 %shard_map.218 = (bf16[64,4096]{1,0:T(8,128)(2,1)}, bf16[64,4096]{1,0:T(8,128)(2,1)}) custom-call(bf16[64,4096]{1,0:T(8,128)(2,1)} %copy-done.12, bf16[64,4096]{1,0:T(8,128)(2,1)} %copy-done.13, bf16[4096,256]{1,0:T(8,128)(2,1)} %refs_2_.3, bf16[4096,256]{1,0:T(8,128)(2,1)} %refs_3_.3, bf16[256,4096]{1,0:T(8,128)(2,1)} %refs_4_.3), custom_call_target="tpu_custom_call" | custom-call | flops 805306368 | bytes 1000000 | tf_op jit(solution)/shard_map/pallas_call | solution.py:160
  241.1 10.2 %shard_map.219 = (bf16[160,4096]{1,0:T(8,128)(2,1)}, bf16[160,4096]{1,0:T(8,128)(2,1)}, bf16[160,4096]{1,0:T(8,128)(2,1)}, bf16[160,4096]{1,0:T(8,128)(2,1)}) custom-call(bf16[160,4096]{1,0:T(8,128)(2,1)} %collective-permute-done.refs_0_, bf16[160,4096]{1,0:T(8,128)(2,1)} %collective-permute-done.8.refs_1_, ...), custom_call_target="tpu_custom_call" | custom-call | flops 4026531840 | bytes 1000000 | tf_op jit(solution)/shard_map/pallas_call | solution.py:160
  251.3 7.4 %shard_map.220 = (bf16[160,4096]{1,0:T(8,128)(2,1)}, bf16[160,4096]{1,0:T(8,128)(2,1)}) custom-call(bf16[160,4096]{1,0:T(8,128)(2,1)} %collective-permute-done.1.refs_0_, bf16[160,4096]{1,0:T(8,128)(2,1)} %collective-permute-done.11.refs_1_, bf16[4096,256]{1,0:T(8,128)(2,1)} %bitcast.183, bf16[4096,256]{1,0:T(8,128)(2,1)} %bitcast.186, ...), custom_call_target="tpu_custom_call" | custom-call | flops 2013265920 | bytes 1000000 | tf_op jit(solution)/shard_map/pallas_call | solution.py:160
  258.7 6.2 %shard_map.221 = (f32[4,512,128]{2,1,0:T(8,128)}, f32[4,512,128]{2,1,0:T(8,128)}, f32[4,512,128]{2,1,0:T(8,128)}) custom-call(s32[1]{0:T(128)} %bitcast.rank_ref, bf16[512,1024]{1,0:T(8,128)(2,1)} %copy.38.q_ref, bf16[18432,512]{1,0:T(8,128)(2,1)} %all-gather.4.cloned.1.call-done.lat_ref, bf16[512,512]{1,0:T(8,128)(2,1)} %wk_ref.7, bf16[512,512]{1,0:T(8,128)(2,1)} %wv_ref.7), custom_call_target="tpu_custom_call" | custom-call | flops 11200000000 | bytes 10000000 | tf_op jit(solution)/shard_map/pallas_call | solution.py:327
  264.9 5.2 shard_map.222
  270.1 5.6 %shard_map.223 = (f32[4,512,128]{2,1,0:T(8,128)}, f32[4,512,128]{2,1,0:T(8,128)}, f32[4,512,128]{2,1,0:T(8,128)}) custom-call(s32[1]{0:T(128)} %bitcast.rank_ref, bf16[512,1024]{1,0:T(8,128)(2,1)} %copy.38.q_ref, bf16[18432,512]{1,0:T(8,128)(2,1)} %all-gather.4.cloned.1.call-done.lat_ref, bf16[512,512]{1,0:T(8,128)(2,1)} %wk_ref.7, bf16[512,512]{1,0:T(8,128)(2,1)} %wv_ref.7, ...), custom_call_target="tpu_custom_call" | custom-call | flops 11200000000 | bytes 10000000 | tf_op jit(solution)/shard_map/pallas_call | solution.py:327
  275.7 4.4 shard_map.224
  280.1 6.7 %convolution_convert_fusion = bf16[512,4096]{1,0:T(8,128)(2,1)} fusion(bf16[512,512]{1,0:T(8,128)(2,1)} %shard_map.224, bf16[512,4096]{1,0:T(8,128)(2,1)} %param.29), kind=kOutput, calls=%fused_computation | convolution fusion | flops 2149580800 | bytes 8912896 | tf_op jit(solution)/shard_map/dot_general | solution.py:467
  286.8 1.3 collective-permute-start.12
  288.1 2.7 collective-permute-start.13
  290.8 3.4 collective-permute-start.15
  294.3 35.3 %collective-permute-done.14 = bf16[64,4096]{1,0:T(8,128)(2,1)S(1)} collective-permute-done((bf16[64,4096]{1,0:T(8,128)(2,1)}, bf16[64,4096]{1,0:T(8,128)(2,1)S(1)}, u32[]{:S(2)}, u32[]{:S(2)}) %collective-permute-start.14) | collective-permute-done | bytes 524320 | tf_op jit(solution)/shard_map/ppermute | solution.py:58
  329.6 1.7 collective-permute-done.15
  332.6 3.7 collective-permute-start.19
  336.7 26.1 %collective-permute-done.17.mh = bf16[160,4096]{1,0:T(8,128)(2,1)S(1)} collective-permute-done((bf16[160,4096]{1,0:T(8,128)(2,1)}, bf16[160,4096]{1,0:T(8,128)(2,1)S(1)}, u32[]{:S(2)}, u32[]{:S(2)}) %collective-permute-start.17) | collective-permute-done | bytes 1310752 | tf_op jit(solution)/shard_map/ppermute | solution.py:58
  362.8 50.9 %collective-permute-done.19.ph = bf16[160,4096]{1,0:T(8,128)(2,1)S(1)} collective-permute-done((bf16[160,4096]{1,0:T(8,128)(2,1)S(1)}, bf16[160,4096]{1,0:T(8,128)(2,1)S(1)}, u32[]{:S(2)}, u32[]{:S(2)}) %collective-permute-start.19) | collective-permute-done | bytes 1310752 | tf_op jit(solution)/shard_map/ppermute | solution.py:62
  413.7 2.9 collective-permute-done.16.ml
  417.8 6.5 %shard_map.225 = bf16[1280,1024]{1,0:T(8,128)(2,1)} custom-call(bf16[160,4096]{1,0:T(8,128)(2,1)} %get-tuple-element.48.ol, bf16[160,4096]{1,0:T(8,128)(2,1)} %get-tuple-element.67.oh, bf16[160,4096]{1,0:T(8,128)(2,1)} %copy-done.10, bf16[160,4096]{1,0:T(8,128)(2,1)} %copy-done.8, bf16[160,4096]{1,0:T(8,128)(2,1)} %copy-done.7, bf16[160,4096]{1,0:T(8,128)(2,1)} %copy-done.9, ...), custom_call_target="tpu_custom_call" | custom-call | flops 2000000000 | bytes 1000000 | tf_op jit(solution)/shard_map/pallas_call | solution.py:462
  424.3 73.5 %all-to-all-start.1 = ((bf16[32,40,1024]{2,1,0:T(8,128)(2,1)}), bf16[32,40,1024]{2,1,0:T(8,128)(2,1)}, u32[]{:S(2)}, u32[]{:S(2)}) async-start(bf16[32,40,1024]{2,1,0:T(8,128)(2,1)} %bitcast.180), calls=%async_computation.2 | async-start | bytes 5242880 | tf_op jit(solution)/shard_map/all_to_all | solution.py:465
  497.9 3.5 collective-permute-start.22
  501.5 3.3 collective-permute-start.23
  506.5 11.2 %collective-permute-done.21.mh = bf16[64,4096]{1,0:T(8,128)(2,1)} collective-permute-done((bf16[64,4096]{1,0:T(8,128)(2,1)}, bf16[64,4096]{1,0:T(8,128)(2,1)}, u32[]{:S(2)}, u32[]{:S(2)}) %collective-permute-start.21) | collective-permute-done | bytes 524320 | tf_op jit(solution)/shard_map/ppermute | solution.py:58
  517.6 6.7 %collective-permute-done.23.ph = bf16[64,4096]{1,0:T(8,128)(2,1)S(1)} collective-permute-done((bf16[64,4096]{1,0:T(8,128)(2,1)S(1)}, bf16[64,4096]{1,0:T(8,128)(2,1)S(1)}, u32[]{:S(2)}, u32[]{:S(2)}) %collective-permute-start.23) | collective-permute-done | bytes 524320 | tf_op jit(solution)/shard_map/ppermute | solution.py:62
  524.3 3.4 collective-permute-done.20.ml
  527.7 6.3 %all-to-all-done.1 = bf16[32,40,1024]{2,1,0:T(8,128)(2,1)} async-done(((bf16[32,40,1024]{2,1,0:T(8,128)(2,1)}), bf16[32,40,1024]{2,1,0:T(8,128)(2,1)}, u32[]{:S(2)}, u32[]{:S(2)}) %all-to-all-start.1) | async-done | bytes 2621472 | tf_op jit(solution)/shard_map/all_to_all | solution.py:465
  534.0 7.2 %shard_map.226 = bf16[128,4096]{1,0:T(8,128)(2,1)} custom-call(bf16[1280,1024]{1,0:T(8,128)(2,1)} %bitcast.55.ret_ref, s32[128,2]{1,0:T(8,128)} %copy.35.routes_ref, f32[128,2]{1,0:T(8,128)} %copy.36.rw_ref, bf16[128,4096]{1,0:T(8,128)(2,1)} %shard_map.215.own, bf16[64,4096]{1,0:T(8,128)(2,1)} %copy-done.23, bf16[64,4096]{1,0:T(8,128)(2,1)} %collective-permute-done.21.mh, ...), custom_call_target="tpu_custom_call" | custom-call | flops 3000000000 | bytes 1000000 | tf_op jit(solution)/shard_map/pallas_call | solution.py:470
  (126 shorter events, 26.6 us)
Async XLA Ops:
  7.2 121.2 %copy-start = (bf16[1024,768]{1,0:T(8,128)(2,1)S(1)}, bf16[1024,768]{1,0:T(8,128)(2,1)}, u32[]{:S(2)}) copy-start(bf16[1024,768]{1,0:T(8,128)(2,1)} %param.26) | copy-start | bytes 4718596
  7.2 33.8 %all-gather.6.cloned.1.call-start = ((), (), s32[]{:S(2)}) async-start(), calls=%async_computation.5 | async-start | bytes 2048000 | tf_op jit(solution)/shard_map/all_gather | solution.py:399
  11.4 247.3 %all-gather.4.cloned.1.call-start = ((), (), s32[]{:S(2)}) async-start(), calls=%async_computation.3 | async-start | bytes 19464192 | tf_op jit(solution)/shard_map/all_gather | solution.py:413
  58.9 7.6 %copy-start.2 = (bf16[128,4096]{1,0:T(8,128)(2,1)S(1)}, bf16[128,4096]{1,0:T(8,128)(2,1)}, u32[]{:S(2)}) copy-start(bf16[128,4096]{1,0:T(8,128)(2,1)} %get-tuple-element.44.refs_0_) | copy-start | bytes 3145732
  59.0 50.2 %all-to-all-start = ((bf16[32,40,1024]{2,1,0:T(8,128)(2,1)}), bf16[32,40,1024]{2,1,0:T(8,128)(2,1)}, u32[]{:S(2)}, u32[]{:S(2)}) async-start(bf16[32,40,1024]{2,1,0:T(8,128)(2,1)} %bitcast.190), calls=%async_computation | async-start | bytes 5242880 | tf_op jit(solution)/shard_map/all_to_all | solution.py:383
  66.5 474.8 %reduce-scatter.2.cloned.1.call-start = ((), (), s32[]{:S(2)}) async-start(), calls=%async_computation.4 | async-start | bytes 5242880 | tf_op jit(solution)/shard_map/reduce_scatter | solution.py:468
  67.6 51.3 %collective-permute-start.2 = (bf16[64,4096]{1,0:T(8,128)(2,1)}, bf16[64,4096]{1,0:T(8,128)(2,1)}, u32[]{:S(2)}, u32[]{:S(2)}) collective-permute-start(bf16[64,4096]{1,0:T(8,128)(2,1)} %get-tuple-element.117), channel_id=1, source_target_pairs={{0,1},{1,2},{2,3},{3,0},{4,5},{5,6},{6,7},{7,4},{8,9},{9,10},{10,1... | collective-permute-start | bytes 1572872 | tf_op jit(solution)/shard_map/ppermute | solution.py:58
  109.1 12.7 %copy-start.3 = (bf16[800,1024]{1,0:T(8,128)(2,1)S(1)}, bf16[800,1024]{1,0:T(8,128)(2,1)}, u32[]{:S(2)}) copy-start(bf16[800,1024]{1,0:T(8,128)(2,1)} %all-gather.6.cloned.1.call-done) | copy-start | bytes 4915204
  113.7 57.4 %collective-permute-start = (bf16[160,4096]{1,0:T(8,128)(2,1)}, bf16[160,4096]{1,0:T(8,128)(2,1)}, u32[]{:S(2)}, u32[]{:S(2)}) collective-permute-start(bf16[160,4096]{1,0:T(8,128)(2,1)} %get-tuple-element.46.refs_0_), channel_id=1, source_target_pairs={{0,1},{1,2},{2,3},{3,0},{4,5},{5,6},{6,7},{7,4},{8,9},{9,10},{10,1... | collective-permute-start | bytes 3932168 | tf_op jit(solution)/shard_map/ppermute | solution.py:58
  115.0 57.2 %collective-permute-start.10 = (bf16[160,4096]{1,0:T(8,128)(2,1)}, bf16[160,4096]{1,0:T(8,128)(2,1)}, u32[]{:S(2)}, u32[]{:S(2)}) collective-permute-start(bf16[160,4096]{1,0:T(8,128)(2,1)} %get-tuple-element.47.refs_1_), channel_id=1, source_target_pairs={{0,3},{1,0},{2,1},{3,2},{4,7},{5,4},{6,5},{7,6},{8,11},{9,8},{10,9... | collective-permute-start | bytes 3932168 | tf_op jit(solution)/shard_map/ppermute | solution.py:62
  116.9 41.3 %collective-permute-start.6 = (bf16[64,4096]{1,0:T(8,128)(2,1)}, bf16[64,4096]{1,0:T(8,128)(2,1)}, u32[]{:S(2)}, u32[]{:S(2)}) collective-permute-start(bf16[64,4096]{1,0:T(8,128)(2,1)} %get-tuple-element.116), channel_id=1, source_target_pairs={{0,3},{1,0},{2,1},{3,2},{4,7},{5,4},{6,5},{7,6},{8,11},{9,8},{10,9... | collective-permute-start | bytes 1572872 | tf_op jit(solution)/shard_map/ppermute | solution.py:62
  118.2 41.5 %collective-permute-start.4 = (bf16[64,4096]{1,0:T(8,128)(2,1)}, bf16[64,4096]{1,0:T(8,128)(2,1)}, u32[]{:S(2)}, u32[]{:S(2)}) collective-permute-start(bf16[64,4096]{1,0:T(8,128)(2,1)} %get-tuple-element.116), channel_id=1, source_target_pairs={{0,1},{1,2},{2,3},{3,0},{4,5},{5,6},{6,7},{7,4},{8,9},{9,10},{10,1... | collective-permute-start | bytes 1572872 | tf_op jit(solution)/shard_map/ppermute | solution.py:58
  118.9 50.5 %collective-permute-start.5 = (bf16[64,4096]{1,0:T(8,128)(2,1)}, bf16[64,4096]{1,0:T(8,128)(2,1)}, u32[]{:S(2)}, u32[]{:S(2)}) collective-permute-start(bf16[64,4096]{1,0:T(8,128)(2,1)} %get-tuple-element.117), channel_id=1, source_target_pairs={{0,3},{1,0},{2,1},{3,2},{4,7},{5,4},{6,5},{7,6},{8,11},{9,8},{10,9... | collective-permute-start | bytes 1572872 | tf_op jit(solution)/shard_map/ppermute | solution.py:62
  128.4 41.0 %copy-start.4 = (bf16[160,4096]{1,0:T(8,128)(2,1)S(1)}, bf16[160,4096]{1,0:T(8,128)(2,1)}, u32[]{:S(2)}) copy-start(bf16[160,4096]{1,0:T(8,128)(2,1)} %get-tuple-element.47.refs_1_) | copy-start | bytes 3932164
  158.2 16.3 %collective-permute-start.3 = (bf16[64,4096]{1,0:T(8,128)(2,1)}, bf16[64,4096]{1,0:T(8,128)(2,1)S(1)}, u32[]{:S(2)}, u32[]{:S(2)}) collective-permute-start(bf16[64,4096]{1,0:T(8,128)(2,1)} %collective-permute-done.2.refs_0_), channel_id=1, source_target_pairs={{0,1},{1,2},{2,3},{3,0},{4,5},{5,6},{6,7},{7,4},{8,9},{9,10},{10,1... | collective-permute-start | bytes 1572872 | tf_op jit(solution)/shard_map/ppermute | solution.py:58
  159.7 81.4 %collective-permute-start.9 = (bf16[160,4096]{1,0:T(8,128)(2,1)}, bf16[160,4096]{1,0:T(8,128)(2,1)}, u32[]{:S(2)}, u32[]{:S(2)}) collective-permute-start(bf16[160,4096]{1,0:T(8,128)(2,1)} %get-tuple-element.46.refs_0_), channel_id=1, source_target_pairs={{0,3},{1,0},{2,1},{3,2},{4,7},{5,4},{6,5},{7,6},{8,11},{9,8},{10,9... | collective-permute-start | bytes 3932168 | tf_op jit(solution)/shard_map/ppermute | solution.py:62
  169.4 71.7 %collective-permute-start.8 = (bf16[160,4096]{1,0:T(8,128)(2,1)S(1)}, bf16[160,4096]{1,0:T(8,128)(2,1)}, u32[]{:S(2)}, u32[]{:S(2)}) collective-permute-start(bf16[160,4096]{1,0:T(8,128)(2,1)S(1)} %copy-done.4), channel_id=1, source_target_pairs={{0,1},{1,2},{2,3},{3,0},{4,5},{5,6},{6,7},{7,4},{8,9},{9,10},{10,1... | collective-permute-start | bytes 3932168 | tf_op jit(solution)/shard_map/ppermute | solution.py:58
  171.0 80.3 %collective-permute-start.1 = (bf16[160,4096]{1,0:T(8,128)(2,1)}, bf16[160,4096]{1,0:T(8,128)(2,1)}, u32[]{:S(2)}, u32[]{:S(2)}) collective-permute-start(bf16[160,4096]{1,0:T(8,128)(2,1)} %collective-permute-done.refs_0_), channel_id=1, source_target_pairs={{0,1},{1,2},{2,3},{3,0},{4,5},{5,6},{6,7},{7,4},{8,9},{9,10},{10,1... | collective-permute-start | bytes 3932168 | tf_op jit(solution)/shard_map/ppermute | solution.py:58
  172.2 79.1 %collective-permute-start.11 = (bf16[160,4096]{1,0:T(8,128)(2,1)}, bf16[160,4096]{1,0:T(8,128)(2,1)}, u32[]{:S(2)}, u32[]{:S(2)}) collective-permute-start(bf16[160,4096]{1,0:T(8,128)(2,1)} %collective-permute-done.10.refs_3_), channel_id=1, source_target_pairs={{0,3},{1,0},{2,1},{3,2},{4,7},{5,4},{6,5},{7,6},{8,11},{9,8},{10,9... | collective-permute-start | bytes 3932168 | tf_op jit(solution)/shard_map/ppermute | solution.py:62
  174.5 9.3 %copy-start.12 = (bf16[64,4096]{1,0:T(8,128)(2,1)}, bf16[64,4096]{1,0:T(8,128)(2,1)S(1)}, u32[]{:S(2)}) copy-start(bf16[64,4096]{1,0:T(8,128)(2,1)S(1)} %collective-permute-done.3.refs_0_) | copy-start | bytes 1572868
  174.5 59.4 %collective-permute-start.7 = (bf16[64,4096]{1,0:T(8,128)(2,1)}, bf16[64,4096]{1,0:T(8,128)(2,1)S(1)}, u32[]{:S(2)}, u32[]{:S(2)}) collective-permute-start(bf16[64,4096]{1,0:T(8,128)(2,1)} %collective-permute-done.6.refs_3_), channel_id=1, source_target_pairs={{0,3},{1,0},{2,1},{3,2},{4,7},{5,4},{6,5},{7,6},{8,11},{9,8},{10,9... | collective-permute-start | bytes 1572872 | tf_op jit(solution)/shard_map/ppermute | solution.py:62
  286.8 1.3 copy-start.21
  286.8 45.4 %copy-start.6 = (bf16[160,4096]{1,0:T(8,128)(2,1)S(1)}, bf16[160,4096]{1,0:T(8,128)(2,1)}, u32[]{:S(2)}) copy-start(bf16[160,4096]{1,0:T(8,128)(2,1)} %get-tuple-element.73) | copy-start | bytes 3932164
  286.8 44.5 %collective-permute-start.12 = (bf16[160,4096]{1,0:T(8,128)(2,1)}, bf16[160,4096]{1,0:T(8,128)(2,1)S(1)}, u32[]{:S(2)}, u32[]{:S(2)}) collective-permute-start(bf16[160,4096]{1,0:T(8,128)(2,1)} %get-tuple-element.56), channel_id=1, source_target_pairs={{0,1},{1,2},{2,3},{3,0},{4,5},{5,6},{6,7},{7,4},{8,9},{9,10},{10,1... | collective-permute-start | bytes 3932168 | tf_op jit(solution)/shard_map/ppermute | solution.py:58
  288.1 43.3 %collective-permute-start.13 = (bf16[160,4096]{1,0:T(8,128)(2,1)S(1)}, bf16[160,4096]{1,0:T(8,128)(2,1)S(1)}, u32[]{:S(2)}, u32[]{:S(2)}) collective-permute-start(bf16[160,4096]{1,0:T(8,128)(2,1)S(1)} %copy-done.21), channel_id=1, source_target_pairs={{0,3},{1,0},{2,1},{3,2},{4,7},{5,4},{6,5},{7,6},{8,11},{9,8},{10,9... | collective-permute-start | bytes 3932168 | tf_op jit(solution)/shard_map/ppermute | solution.py:62
  290.8 38.8 %collective-permute-start.14 = (bf16[64,4096]{1,0:T(8,128)(2,1)}, bf16[64,4096]{1,0:T(8,128)(2,1)S(1)}, u32[]{:S(2)}, u32[]{:S(2)}) collective-permute-start(bf16[64,4096]{1,0:T(8,128)(2,1)} %get-tuple-element.52), channel_id=1, source_target_pairs={{0,1},{1,2},{2,3},{3,0},{4,5},{5,6},{6,7},{7,4},{8,9},{9,10},{10,1... | collective-permute-start | bytes 1572872 | tf_op jit(solution)/shard_map/ppermute | solution.py:58
  290.8 40.5 %collective-permute-start.15 = (bf16[64,4096]{1,0:T(8,128)(2,1)}, bf16[64,4096]{1,0:T(8,128)(2,1)S(1)}, u32[]{:S(2)}, u32[]{:S(2)}) collective-permute-start(bf16[64,4096]{1,0:T(8,128)(2,1)} %get-tuple-element.70), channel_id=1, source_target_pairs={{0,3},{1,0},{2,1},{3,2},{4,7},{5,4},{6,5},{7,6},{8,11},{9,8},{10,9... | collective-permute-start | bytes 1572872 | tf_op jit(solution)/shard_map/ppermute | solution.py:62
  294.2 68.6 %collective-permute-start.18 = (bf16[160,4096]{1,0:T(8,128)(2,1)}, bf16[160,4096]{1,0:T(8,128)(2,1)S(1)}, u32[]{:S(2)}, u32[]{:S(2)}) collective-permute-start(bf16[160,4096]{1,0:T(8,128)(2,1)} %get-tuple-element.54), channel_id=1, source_target_pairs={{0,3},{1,0},{2,1},{3,2},{4,7},{5,4},{6,5},{7,6},{8,11},{9,8},{10,9... | collective-permute-start | bytes 3932168 | tf_op jit(solution)/shard_map/ppermute | solution.py:62
  329.6 33.2 %collective-permute-start.17 = (bf16[160,4096]{1,0:T(8,128)(2,1)}, bf16[160,4096]{1,0:T(8,128)(2,1)S(1)}, u32[]{:S(2)}, u32[]{:S(2)}) collective-permute-start(bf16[160,4096]{1,0:T(8,128)(2,1)} %get-tuple-element.72), channel_id=1, source_target_pairs={{0,1},{1,2},{2,3},{3,0},{4,5},{5,6},{6,7},{7,4},{8,9},{9,10},{10,1... | collective-permute-start | bytes 3932168 | tf_op jit(solution)/shard_map/ppermute | solution.py:58
  332.1 4.1 copy-start.5
  332.6 81.2 %collective-permute-start.19 = (bf16[160,4096]{1,0:T(8,128)(2,1)S(1)}, bf16[160,4096]{1,0:T(8,128)(2,1)S(1)}, u32[]{:S(2)}, u32[]{:S(2)}) collective-permute-start(bf16[160,4096]{1,0:T(8,128)(2,1)S(1)} %add_convert_fusion), channel_id=1, source_target_pairs={{0,3},{1,0},{2,1},{3,2},{4,7},{5,4},{6,5},{7,6},{8,11},{9,8},{10,9... | collective-permute-start | bytes 3932168 | tf_op jit(solution)/shard_map/ppermute | solution.py:62
  336.6 80.0 %collective-permute-start.16 = (bf16[160,4096]{1,0:T(8,128)(2,1)S(1)}, bf16[160,4096]{1,0:T(8,128)(2,1)S(1)}, u32[]{:S(2)}, u32[]{:S(2)}) collective-permute-start(bf16[160,4096]{1,0:T(8,128)(2,1)S(1)} %add_convert_fusion.1), channel_id=1, source_target_pairs={{0,1},{1,2},{2,3},{3,0},{4,5},{5,6},{6,7},{7,4},{8,9},{9,10},{10,1... | collective-permute-start | bytes 3932168 | tf_op jit(solution)/shard_map/ppermute | solution.py:58
  362.8 53.8 %copy-start.8 = (bf16[160,4096]{1,0:T(8,128)(2,1)}, bf16[160,4096]{1,0:T(8,128)(2,1)S(1)}, u32[]{:S(2)}) copy-start(bf16[160,4096]{1,0:T(8,128)(2,1)S(1)} %collective-permute-done.17.mh) | copy-start | bytes 3932164
  362.8 53.8 %copy-start.7 = (bf16[160,4096]{1,0:T(8,128)(2,1)}, bf16[160,4096]{1,0:T(8,128)(2,1)S(1)}, u32[]{:S(2)}) copy-start(bf16[160,4096]{1,0:T(8,128)(2,1)S(1)} %collective-permute-done.18.pl_) | copy-start | bytes 3932164
  413.7 2.9 copy-start.9
  424.3 77.1 %copy-start.15 = (bf16[64,4096]{1,0:T(8,128)(2,1)S(1)}, bf16[64,4096]{1,0:T(8,128)(2,1)}, u32[]{:S(2)}) copy-start(bf16[64,4096]{1,0:T(8,128)(2,1)} %get-tuple-element.78) | copy-start | bytes 1572868
  424.3 77.1 %copy-start.17 = (bf16[64,4096]{1,0:T(8,128)(2,1)S(1)}, bf16[64,4096]{1,0:T(8,128)(2,1)}, u32[]{:S(2)}) copy-start(bf16[64,4096]{1,0:T(8,128)(2,1)} %copy-done.16) | copy-start | bytes 1572868
  424.3 109.7 %all-to-all-start.1 = ((bf16[32,40,1024]{2,1,0:T(8,128)(2,1)}), bf16[32,40,1024]{2,1,0:T(8,128)(2,1)}, u32[]{:S(2)}, u32[]{:S(2)}) async-start(bf16[32,40,1024]{2,1,0:T(8,128)(2,1)} %bitcast.180), calls=%async_computation.2 | async-start | bytes 5242880 | tf_op jit(solution)/shard_map/all_to_all | solution.py:465
  497.8 6.9 %copy-start.14 = (bf16[64,4096]{1,0:T(8,128)(2,1)S(1)}, bf16[64,4096]{1,0:T(8,128)(2,1)}, u32[]{:S(2)}) copy-start(bf16[64,4096]{1,0:T(8,128)(2,1)} %get-tuple-element.75) | copy-start | bytes 1572868
  497.8 7.1 %copy-start.19 = (s32[128,2]{0,1:T(2,128)S(1)}, s32[128,2]{0,1:T(2,128)}, u32[]{:S(2)}) copy-start(s32[128,2]{0,1:T(2,128)} %param.32) | copy-start | bytes 3076
  497.8 7.9 %copy-start.20 = (f32[128,2]{0,1:T(2,128)S(1)}, f32[128,2]{0,1:T(2,128)}, u32[]{:S(2)}) copy-start(f32[128,2]{0,1:T(2,128)} %param.33) | copy-start | bytes 3076
  497.9 19.8 %collective-permute-start.22 = (bf16[64,4096]{1,0:T(8,128)(2,1)}, bf16[64,4096]{1,0:T(8,128)(2,1)}, u32[]{:S(2)}, u32[]{:S(2)}) collective-permute-start(bf16[64,4096]{1,0:T(8,128)(2,1)} %get-tuple-element.50), channel_id=1, source_target_pairs={{0,3},{1,0},{2,1},{3,2},{4,7},{5,4},{6,5},{7,6},{8,11},{9,8},{10,9... | collective-permute-start | bytes 1572872 | tf_op jit(solution)/shard_map/ppermute | solution.py:62
  501.3 16.3 %collective-permute-start.21 = (bf16[64,4096]{1,0:T(8,128)(2,1)}, bf16[64,4096]{1,0:T(8,128)(2,1)}, u32[]{:S(2)}, u32[]{:S(2)}) collective-permute-start(bf16[64,4096]{1,0:T(8,128)(2,1)} %get-tuple-element.77), channel_id=1, source_target_pairs={{0,1},{1,2},{2,3},{3,0},{4,5},{5,6},{6,7},{7,4},{8,9},{9,10},{10,1... | collective-permute-start | bytes 1572872 | tf_op jit(solution)/shard_map/ppermute | solution.py:58
  501.5 22.9 %collective-permute-start.23 = (bf16[64,4096]{1,0:T(8,128)(2,1)S(1)}, bf16[64,4096]{1,0:T(8,128)(2,1)S(1)}, u32[]{:S(2)}, u32[]{:S(2)}) collective-permute-start(bf16[64,4096]{1,0:T(8,128)(2,1)S(1)} %add_convert_fusion.2), channel_id=1, source_target_pairs={{0,3},{1,0},{2,1},{3,2},{4,7},{5,4},{6,5},{7,6},{8,11},{9,8},{10,9... | collective-permute-start | bytes 1572872 | tf_op jit(solution)/shard_map/ppermute | solution.py:62
  504.9 22.8 %collective-permute-start.20 = (bf16[64,4096]{1,0:T(8,128)(2,1)S(1)}, bf16[64,4096]{1,0:T(8,128)(2,1)S(1)}, u32[]{:S(2)}, u32[]{:S(2)}) collective-permute-start(bf16[64,4096]{1,0:T(8,128)(2,1)S(1)} %add_convert_fusion.3), channel_id=1, source_target_pairs={{0,1},{1,2},{2,3},{3,0},{4,5},{5,6},{6,7},{7,4},{8,9},{9,10},{10,1... | collective-permute-start | bytes 1572872 | tf_op jit(solution)/shard_map/ppermute | solution.py:58
  524.3 3.4 copy-start.22
  527.7 6.3 %copy-start.23 = (bf16[64,4096]{1,0:T(8,128)(2,1)}, bf16[64,4096]{1,0:T(8,128)(2,1)S(1)}, u32[]{:S(2)}) copy-start(bf16[64,4096]{1,0:T(8,128)(2,1)S(1)} %collective-permute-done.20.ml) | copy-start | bytes 1572868
  534.0 7.2 %copy-start.1 = (bf16[1024,768]{1,0:T(8,128)(2,1)S(1)}, bf16[1024,768]{1,0:T(8,128)(2,1)}, u32[]{:S(2)}) copy-start(bf16[1024,768]{1,0:T(8,128)(2,1)} %param.26) | copy-start | bytes 4718596
  (5 other events, 4.2 us)
Sparse Core Ops, SparseCore 0:
  11.5 29.4 all-gather.5
  54.3 103.6 all-gather.3
  286.9 136.4 reduce-scatter.1
